TPU v7x, 1024 devices: a whole 8x8x8 slice. The times are simulated.
1024 devices in a mesh: ep: 64 (over z, y), tp: 16 (over x, core).
Axes of the slice: x: 8, y: 8, z: 8, core: 2. Of those that a mesh axis runs over, the one named last changes fastest.
Arguments:
- tokens: bfloat16 [2048, 4096], P('ep', 'tp')
- norm_gain: float32 [4096], P('tp'), may hold values from 0.1 to 1.9
- routes: int32 [2048, 8], P('ep'), may hold values from 0 to 63, all different within a row; in each aligned block of 32 rows (0 to 31, 32 to 63, ...) at most 6 rows name the same one
- route_weights: float32 [2048, 8], P('ep'), may hold values from 0.1 to 1
- gate_proj: bfloat16 [64, 4096, 1024], P('ep', 'tp'), may hold values from -0.09375 to 0.09375
- up_proj: bfloat16 [64, 4096, 1024], P('ep', 'tp'), may hold values from -0.09375 to 0.09375
- down_proj: bfloat16 [64, 1024, 4096], P('ep', None, 'tp')
- shared_gate: bfloat16 [4096, 1024], P('tp'), may hold values from -0.09375 to 0.09375
- shared_up: bfloat16 [4096, 1024], P('tp'), may hold values from -0.09375 to 0.09375
- shared_down: bfloat16 [1024, 4096], P(None, 'tp')
- out_gain: float32 [4096], P('tp'), may hold values from 0.1 to 1.9
Outputs:
- mixed_out: bfloat16 [2048, 4096], P('ep', 'tp')
Inputs may be any that keep to these rules, and one draw needn't show every extreme that they name: `routes`: among the 32 rows of one device no expert is named more than 6 times, and in every draw some expert is named exactly 6 times by the rows of some device.
All inputs are finite; a program needn't handle non-finite values.
Results may differ from a plain program's by a relative error of at most 0.028.
Values may be sent and summed in bfloat16 or wider, within the bound.
No kernel may reach another device: no remote copies, remote signals or barrier semaphores. Data moves between devices by JAX's collectives and lax.ppermute only.
A program may use at most 32 MiB of HBM per device.

v0:
```python
import jax
import jax.numpy as jnp
from jax import lax
from jax.sharding import PartitionSpec as P

D = 4096


def sent_to_all(array, axis):
    devices = lax.axis_size(axis)
    return lax.all_to_all(
        jnp.broadcast_to(array[None], (devices, *array.shape)), axis, 0, 0, tiled=True
    )


def over_copies(array, axis):
    everything = sent_to_all(array, axis)
    return jnp.sum(everything, axis=0)


def split_up(array, dim, devices):
    lengths = array.shape
    blocks = array.reshape(*lengths[:dim], devices, lengths[dim] // devices, *lengths[dim + 1 :])
    return jnp.moveaxis(blocks, dim, 0)


def one_scatter(arrays, axis, dims):
    devices = lax.axis_size(axis)
    blocks = [split_up(a, dim, devices) for a, dim in zip(arrays, dims)]
    lines = jnp.concatenate([b.reshape(devices, -1) for b in blocks], axis=1)
    extent = max(16, -(-lines.shape[1] // 1024) * 8)
    lines = jnp.pad(lines, ((0, 0), (0, extent * 128 - lines.shape[1]))).reshape(-1, 128)
    line, at, outs = (lax.psum_scatter(lines, axis, tiled=True).reshape(-1), 0, [])
    for b in blocks:
        part = b[0]
        outs.append(line[at : at + part.size].reshape(part.shape))
        at += part.size
    return tuple(outs)


def gather_turned(arrays, axis, dims):
    turned = [jnp.moveaxis(a, dim, 0) for a, dim in zip(arrays, dims)]
    widths = [t[0].size for t in turned]
    both = jnp.concatenate([t.reshape(-1, w) for t, w in zip(turned, widths)], axis=1)
    whole = lax.all_gather(both, axis, axis=0, tiled=True)
    blocks = jnp.split(whole, [sum(widths[:k]) for k in range(1, len(widths))], axis=1)
    return tuple(
        (
            jnp.moveaxis(b.reshape(-1, *t.shape[1:]), 0, dim)
            for b, t, dim in zip(blocks, turned, dims)
        )
    )


def per_device(
    tokens,
    norm_gain,
    routes,
    route_weights,
    gate_proj,
    up_proj,
    down_proj,
    shared_gate,
    shared_up,
    shared_down,
    out_gain,
):
    tokens_f = tokens.astype(jnp.float32)
    squares = over_copies(jnp.sum(tokens_f * tokens_f, axis=1), "tp")
    normed = (tokens_f * lax.rsqrt(squares / D + 1e-06)[:, None] * norm_gain[None, :]).astype(
        jnp.bfloat16
    )
    tok_rows, picks = routes.shape
    feat_local = tokens.shape[1]
    sources = lax.axis_size("ep")
    exp_local = gate_proj.shape[0]
    experts_all = sources * exp_local
    capacity = min(
        tok_rows, max(2, (3 * tok_rows * picks + 2 * experts_all - 1) // (2 * experts_all))
    )
    chosen = routes.reshape(-1)
    assigned = chosen.shape[0]
    earlier = jnp.arange(assigned)[None, :] < jnp.arange(assigned)[:, None]
    matches = (chosen[:, None] == chosen[None, :]) & earlier
    slot_rank = jnp.sum(matches.astype(jnp.int32), axis=1)
    slot_index = chosen * capacity + slot_rank
    source_rows = jnp.repeat(normed, picks, axis=0)
    outgoing = (
        jnp.zeros((experts_all * capacity, feat_local), jnp.bfloat16)
        .at[slot_index]
        .set(source_rows)
    )
    outgoing = outgoing.reshape(sources, exp_local, capacity, feat_local)
    arrived = lax.all_to_all(outgoing, "ep", split_axis=0, concat_axis=0, tiled=True)
    gate_part = jnp.einsum("sjcd,jdf->sjcf", arrived, gate_proj, preferred_element_type=jnp.float32)
    up_part = jnp.einsum("sjcd,jdf->sjcf", arrived, up_proj, preferred_element_type=jnp.float32)
    shared_gate_part = jnp.dot(normed, shared_gate, preferred_element_type=jnp.float32).reshape(
        1, 1, tok_rows, -1
    )
    shared_up_part = jnp.dot(normed, shared_up, preferred_element_type=jnp.float32).reshape(
        1, 1, tok_rows, -1
    )
    gate_pre, up_pre, shared_gate_pre, shared_up_pre = tuple(
        (
            part.astype(jnp.float32)
            for part in one_scatter(
                (
                    gate_part.astype(jnp.bfloat16),
                    up_part.astype(jnp.bfloat16),
                    shared_gate_part.astype(jnp.bfloat16),
                    shared_up_part.astype(jnp.bfloat16),
                ),
                "tp",
                (3, 3, 3, 3),
            )
        )
    )
    hidden_piece = (jax.nn.silu(gate_pre) * up_pre).astype(jnp.bfloat16)
    shared_piece = (jax.nn.silu(shared_gate_pre) * shared_up_pre).astype(jnp.bfloat16)
    hidden, shared_hidden = gather_turned((hidden_piece, shared_piece), "tp", (3, 3))
    expert_rows = jnp.einsum(
        "sjcf,jfd->sjcd", hidden, down_proj, preferred_element_type=jnp.float32
    ).astype(jnp.bfloat16)
    returned = lax.all_to_all(expert_rows, "ep", split_axis=0, concat_axis=0, tiled=True)
    returned = returned.reshape(experts_all * capacity, feat_local)
    gathered = returned[slot_index].astype(jnp.float32).reshape(tok_rows, picks, feat_local)
    routed = jnp.sum(gathered * route_weights[:, :, None], axis=1)
    shared_part = jnp.dot(
        shared_hidden.reshape(tok_rows, -1), shared_down, preferred_element_type=jnp.float32
    )
    mixed = shared_part + routed
    final_squares = over_copies(jnp.sum(mixed * mixed, axis=1), "tp")
    return (mixed * lax.rsqrt(final_squares / D + 1e-06)[:, None] * out_gain[None, :]).astype(
        jnp.bfloat16
    )


def solution(mesh):
    return jax.shard_map(
        per_device,
        mesh=mesh,
        in_specs=(
            P("ep", "tp"),
            P("tp"),
            P("ep", None),
            P("ep", None),
            P("ep", "tp", None),
            P("ep", "tp", None),
            P("ep", None, "tp"),
            P("tp", None),
            P("tp", None),
            P(None, "tp"),
            P("tp"),
        ),
        out_specs=P("ep", "tp"),
        check_vma=False,
    )
```

profile of v0, /device:TPU:1, one launch (start us, length us, event | category | flops | bytes accessed | tf_op | source)
XLA Modules:
  0.0 208.6 jit_solution(10613754452660749432)
XLA Ops:
  6.5 0.9 fusion.19
  7.5 0.6 broadcast_in_dim.9
  8.1 17.4 %all-to-all-start = ((f32[16,1,32]{2,1,0:T(1,128)}), f32[16,1,32]{2,1,0:T(1,128)S(1)}, u32[]{:S(2)}, u32[]{:S(2)}) async-start(f32[16,1,32]{2,1,0:T(1,128)} %broadcast_in_dim.9), calls=%async_computation | async-start | bytes 16384 | tf_op jit(solution)/shard_map/all_to_all | solution.py:11
  25.4 0.7 broadcast_multiply_fusion
  26.1 0.8 copy.50
  27.0 0.1 mul.110
  27.1 0.2 convert_reduce_fusion
  27.3 5.1 %all-to-all-done = f32[16,1,32]{2,1,0:T(1,128)S(1)} async-done(((f32[16,1,32]{2,1,0:T(1,128)}), f32[16,1,32]{2,1,0:T(1,128)S(1)}, u32[]{:S(2)}, u32[]{:S(2)}) %all-to-all-start) | async-done | bytes 2080 | tf_op jit(solution)/shard_map/all_to_all | solution.py:11
  32.5 0.8 fusion.21
  33.3 1.5 scatter_custom_fusion
  34.8 0.8 reshape.265
  35.6 14.0 %all-to-all-start.1 = ((bf16[64,1,6,256]{3,2,1,0:T(8,128)(2,1)}), bf16[64,1,6,256]{3,2,1,0:T(8,128)(2,1)S(1)}, u32[]{:S(2)}, u32[]{:S(2)}) async-start(bf16[64,1,6,256]{3,2,1,0:T(8,128)(2,1)} %bitcast.4), calls=%async_computation.1 | async-start | bytes 524288 | tf_op jit(solution)/shard_map/all_to_all | solution.py:94
  49.6 1.2 convolution_convert_fusion.4
  50.8 0.2 reshape.273
  51.0 0.2 reshape.274
  51.2 0.2 convolution_convert_fusion.3
  51.4 0.2 reshape.275
  51.6 0.2 reshape.276
  51.8 10.6 %all-to-all-done.1 = bf16[64,1,6,256]{3,2,1,0:T(8,128)(2,1)S(1)} async-done(((bf16[64,1,6,256]{3,2,1,0:T(8,128)(2,1)}), bf16[64,1,6,256]{3,2,1,0:T(8,128)(2,1)S(1)}, u32[]{:S(2)}, u32[]{:S(2)}) %all-to-all-start.1) | async-done | bytes 196640 | tf_op jit(solution)/shard_map/all_to_all | solution.py:94
  62.4 0.4 fusion
  62.8 0.3 copy-done.1
  63.1 1.9 reshape.268
  65.0 2.5 %copy.81 = bf16[64,1,6,16,64]{4,2,0,3,1:T(8,128)(2,1)S(1)} copy(bf16[64,1,6,16,64]{4,3,0,2,1:T(8,128)(2,1)} %reshape.268) | data formatting | bytes 1572864 | tf_op jit(solution)/shard_map/reshape | solution.py:23
  67.5 1.7 reshape.269
  69.2 1.5 fusion.1
  70.7 1.9 reshape.271
  72.6 2.5 %copy.80 = bf16[64,1,6,16,64]{4,2,0,3,1:T(8,128)(2,1)S(1)} copy(bf16[64,1,6,16,64]{4,3,0,2,1:T(8,128)(2,1)} %reshape.271) | data formatting | bytes 1572864 | tf_op jit(solution)/shard_map/reshape | solution.py:23
  75.1 2.4 %reshape.272 = bf16[16,24576]{1,0:T(8,128)(2,1)} reshape(bf16[16,64,1,6,64]{4,3,1,0,2:T(8,128)(2,1)S(1)} %bitcast.108) | data formatting | bytes 1572864 | tf_op jit(solution)/shard_map/reshape | solution.py:30
  77.5 1.2 pad_maximum_fusion
  78.7 1.7 reshape.277
  80.5 53.6 %reduce-scatter.2.cloned.1.call-done = bf16[416,128]{1,0:T(8,128)(2,1)} async-done(((bf16[6656,128]{1,0:T(8,128)(2,1)}), bf16[416,128]{1,0:T(8,128)(2,1)}) %reduce-scatter.2.cloned.1.call-update) | async-done | bytes 106512 | tf_op jit(solution)/shard_map/reduce_scatter | solution.py:33
  134.0 0.8 slice_convert_fusion.1
  134.9 0.1 reshape.286
  135.0 0.1 reshape.287
  135.2 0.7 slice_convert_fusion.3
  136.1 0.1 copy.58
  136.2 18.4 %all_gather.3 = bf16[1024,416]{1,0:T(8,128)(2,1)S(1)} all-gather(bf16[64,416]{1,0:T(8,128)(2,1)S(1)} %copy.58), channel_id=1, replica_groups=mesh['ep'=64,'tp'=16] {'tp'}, dimensions={0}, use_global_device_ids=true | all-gather | bytes 905216 | tf_op jit(solution)/shard_map/all_gather | solution.py:45
  154.7 0.3 copy.59
  155.0 0.3 reshape.282
  155.3 2.0 fusion.2
  157.3 0.8 copy.61
  158.1 14.2 %all-to-all-start.2 = ((bf16[64,1,6,256]{3,2,1,0:T(8,128)(2,1)}), bf16[64,1,6,256]{3,2,1,0:T(8,128)(2,1)S(1)}, u32[]{:S(2)}, u32[]{:S(2)}) async-start(bf16[64,1,6,256]{3,2,1,0:T(8,128)(2,1)} %copy.61), calls=%async_computation.3 | async-start | bytes 524288 | tf_op jit(solution)/shard_map/all_to_all | solution.py:124
  172.4 13.3 %all-to-all-done.2 = bf16[64,1,6,256]{3,2,1,0:T(8,128)(2,1)S(1)} async-done(((bf16[64,1,6,256]{3,2,1,0:T(8,128)(2,1)}), bf16[64,1,6,256]{3,2,1,0:T(8,128)(2,1)S(1)}, u32[]{:S(2)}, u32[]{:S(2)}) %all-to-all-start.2) | async-done | bytes 196640 | tf_op jit(solution)/shard_map/all_to_all | solution.py:124
  185.8 1.2 gather_fusion
  186.9 0.1 fusion.8
  187.1 0.3 multiply_reduce_fusion
  187.4 13.6 %all_to_all.22 = f32[16,1,32]{2,1,0:T(1,128)S(1)} all-to-all(f32[16,1,32]{2,1,0:T(1,128)S(1)} %broadcast_in_dim.11), channel_id=1, replica_groups=mesh['ep'=64,'tp'=16] {'tp'}, dimensions={0} | all-to-all | bytes 4096 | tf_op jit(solution)/shard_map/all_to_all | solution.py:11
  201.1 0.7 multiply_convert_fusion.1
  (33 shorter events, 0.9 us)
Async XLA Ops:
  6.5 55.9 %copy-start = (bf16[1,256,1024]{2,1,0:T(8,128)(2,1)S(1)}, bf16[1,256,1024]{2,1,0:T(8,128)(2,1)}, u32[]{:S(2)}) copy-start(bf16[1,256,1024]{2,1,0:T(8,128)(2,1)} %param.15) | copy-start | bytes 1572868
  6.5 44.7 %copy-start.2 = (bf16[256,1024]{1,0:T(8,128)(2,1)S(1)}, bf16[256,1024]{1,0:T(8,128)(2,1)}, u32[]{:S(2)}) copy-start(bf16[256,1024]{1,0:T(8,128)(2,1)} %param.19) | copy-start | bytes 1572868
  8.1 24.4 %all-to-all-start = ((f32[16,1,32]{2,1,0:T(1,128)}), f32[16,1,32]{2,1,0:T(1,128)S(1)}, u32[]{:S(2)}, u32[]{:S(2)}) async-start(f32[16,1,32]{2,1,0:T(1,128)} %broadcast_in_dim.9), calls=%async_computation | async-start | bytes 16384 | tf_op jit(solution)/shard_map/all_to_all | solution.py:11
  35.6 26.8 %all-to-all-start.1 = ((bf16[64,1,6,256]{3,2,1,0:T(8,128)(2,1)}), bf16[64,1,6,256]{3,2,1,0:T(8,128)(2,1)S(1)}, u32[]{:S(2)}, u32[]{:S(2)}) async-start(bf16[64,1,6,256]{3,2,1,0:T(8,128)(2,1)} %bitcast.4), calls=%async_computation.1 | async-start | bytes 524288 | tf_op jit(solution)/shard_map/all_to_all | solution.py:94
  49.6 84.5 %reduce-scatter.2.cloned.1.call-start = ((), (), s32[]{:S(2)}) async-start(), calls=%async_computation.5 | async-start | bytes 1810432 | tf_op jit(solution)/shard_map/reduce_scatter | solution.py:33
  62.4 0.7 copy-start.1
  155.2 17.0 %copy-start.4 = (f32[32,8]{0,1:T(8,128)S(1)}, f32[32,8]{0,1:T(8,128)}, u32[]{:S(2)}) copy-start(f32[32,8]{0,1:T(8,128)} %param.14) | copy-start | bytes 3076
  157.3 29.8 %copy-start.3 = (bf16[1024,256]{1,0:T(8,128)(2,1)S(1)}, bf16[1024,256]{1,0:T(8,128)(2,1)}, u32[]{:S(2)}) copy-start(bf16[1024,256]{1,0:T(8,128)(2,1)} %param.20) | copy-start | bytes 1572868
  158.1 43.0 %copy-start.5 = (f32[256]{0:T(256)S(1)}, f32[256]{0:T(256)}, u32[]{:S(2)}) copy-start(f32[256]{0:T(256)} %param.21) | copy-start | bytes 3076
  158.1 27.6 %all-to-all-start.2 = ((bf16[64,1,6,256]{3,2,1,0:T(8,128)(2,1)}), bf16[64,1,6,256]{3,2,1,0:T(8,128)(2,1)S(1)}, u32[]{:S(2)}, u32[]{:S(2)}) async-start(bf16[64,1,6,256]{3,2,1,0:T(8,128)(2,1)} %copy.61), calls=%async_computation.3 | async-start | bytes 524288 | tf_op jit(solution)/shard_map/all_to_all | solution.py:124
Sparse Core Ops, SparseCore 0:
  80.6 53.3 reduce-scatter.1
where the time goes:
time: 209 us
  waiting for transfers between devices  82.6 us (40%)
  starting transfers between devices  45.6 us (22%)
  blocking collectives  32 us (15%)
  local copies, waits for them, and re-layouts  22.8 us (11%)
  between operations  13.6 us (7%)
  other arithmetic  6.38 us (3%)
  matrix products  5.62 us (3%)
    reduce_scatter x1, waiting for transfers between devices, one_scatter(): lax.psum_scatter(lines, axis, tiled=True).reshape(-1)  53.6 us
    all_gather x1, blocking collectives, gather_turned(): whole = lax.all_gather(both, axis, axis=0, tiled=True)  18.4 us
    all_to_all x1, starting transfers between devices, sent_to_all(): lax.all_to_all(jnp.broadcast_to(array[None], (devices, *array.shape)), ax...  17.4 us
    all_to_all x1, starting transfers between devices, per_device(): lax.all_to_all(expert_rows, 'ep', split_axis=0, concat_axis=0, tiled=True)  14.2 us
    all_to_all x1, starting transfers between devices, per_device(): lax.all_to_all(outgoing, 'ep', split_axis=0, concat_axis=0, tiled=True)  14 us
    all_to_all x1, blocking collectives, sent_to_all(): lax.all_to_all(jnp.broadcast_to(array[None], (devices, *array.shape)), ax...  13.6 us
    all_to_all x1, waiting for transfers between devices, per_device(): lax.all_to_all(expert_rows, 'ep', split_axis=0, concat_axis=0, tiled=True)  13.3 us
    all_to_all x1, waiting for transfers between devices, per_device(): lax.all_to_all(outgoing, 'ep', split_axis=0, concat_axis=0, tiled=True)  10.6 us
  transfers between devices with their start and end apart: 4, of which 4 were waited for; matrix products, arithmetic and copies ran while one was open for 2% of the time, Pallas kernels for 0%

commit v1 on v0

v1 whole, which is shorter than its diff:
```python
import jax
import jax.numpy as jnp
from jax import lax
from jax.experimental import pallas as pl
from jax.experimental.pallas import tpu as pltpu
from jax.sharding import Mesh, PartitionSpec as P

D = 4096
EPS = 1e-06
bf16, f32, i32 = jnp.bfloat16, jnp.float32, jnp.int32
MIB = 1024 * 1024


def iota(shape, dim):
    return lax.broadcasted_iota(i32, shape, dim)


def dot(a, b):
    return jnp.dot(a, b, preferred_element_type=f32)


def to_row(column, lanes):
    rows = column.shape[0]
    own = iota((rows, lanes), 0) == iota((rows, lanes), 1)
    return jnp.sum(jnp.where(own, column, 0.0), axis=0, keepdims=True)


def to_column(row, rows):
    lanes = row.shape[1]
    own = iota((rows, lanes), 0) == iota((rows, lanes), 1)
    return jnp.sum(jnp.where(own, row, 0.0), axis=1, keepdims=True)


def three_parts(value):
    high = value.astype(bf16).astype(f32)
    rest = jnp.where(high < jnp.inf, value - high, 0.0)
    middle = rest.astype(bf16).astype(f32)
    return high, middle, rest - middle


def named_slots(routes, lanes):
    rows, picks = routes.shape
    expert = iota((rows, lanes), 1) >> 3
    named = routes[:, 0:1] == expert
    for k in range(1, picks):
        named = named | (routes[:, k : k + 1] == expert)
    earlier = (iota((rows, rows), 1) < iota((rows, rows), 0)).astype(f32).astype(bf16)
    rank = dot(earlier, jnp.where(named, 1.0, 0.0).astype(bf16))
    return named, rank.astype(i32)


def pack_kernel(core_ref, routes_ref, own_ref, both_ref, out_ref):
    core = core_ref[0]
    lanes = out_ref.shape[0]
    named, rank = named_slots(routes_ref[...], lanes)
    lane = iota(named.shape, 1)
    slot = lane & 3
    chosen = named & (rank == 3 * core + slot) & (slot < 3)
    other = (lane & 4) > 0
    picks = jnp.concatenate(
        [
            jnp.where(chosen & ~other, 1.0, 0.0).astype(bf16),
            jnp.where(chosen & other, 1.0, 0.0).astype(bf16),
        ],
        axis=0,
    )
    rows = jnp.concatenate([own_ref[...], both_ref[1 - core]], axis=0)
    out_ref[...] = lax.dot_general(
        picks, rows, (((0,), (0,)), ((), ())), preferred_element_type=f32
    ).astype(bf16)


def weights_kernel(routes_ref, weights_ref, out_ref):
    routes = routes_ref[...]
    lanes = out_ref.shape[2]
    named, rank = named_slots(routes, lanes)
    lane = iota(named.shape, 1)
    weight = jnp.zeros(named.shape, f32)
    for k in range(routes.shape[1]):
        weight = jnp.where(routes[:, k : k + 1] == lane >> 3, weights_ref[:, k : k + 1], weight)
    weight = jnp.where(named & (rank == (lane & 7)), weight, 0.0)
    for n, part in enumerate(three_parts(weight)):
        out_ref[n] = part.astype(bf16)


def shared_up_kernel(core_ref, own_ref, gain_ref, gate_ref, up_ref, keep_ref, send_ref):
    first = core_ref[0] == 0
    rows = (own_ref[...].astype(f32) * gain_ref[...]).astype(bf16)
    half = rows.shape[0] // 2
    for n in range(keep_ref.shape[0]):
        cut = slice(n * 128, (n + 1) * 128)
        part = dot(rows, jnp.concatenate([gate_ref[:, cut], up_ref[:, cut]], axis=1))
        keep_ref[n] = jnp.where(first, part[:half], part[half:])
        send_ref[n] = jnp.where(first, part[half:], part[:half]).astype(bf16)


def hidden_parts_kernel(
    core_ref,
    rows_ref,
    both_ref,
    gain_ref,
    gain_other_ref,
    gate_ref,
    up_ref,
    gate_other_ref,
    up_other_ref,
    kept_ref,
    sent_ref,
    out_ref,
):
    first = core_ref[0] == 0
    arrived = rows_ref[...]
    slots = 3 * arrived.shape[0] // 8
    sources = arrived.shape[0] // 8
    to, at = iota((slots, arrived.shape[0]), 0), iota((slots, arrived.shape[0]), 1)
    place = (to % sources) * 8 + to // sources
    own = dot(jnp.where(at == place, 1.0, 0.0).astype(bf16), arrived)
    other = dot(jnp.where(at == place + 4, 1.0, 0.0).astype(bf16), arrived)
    squares = jnp.sum(own * own + other * other, axis=1, keepdims=True)
    near, far = both_ref[0].astype(f32), both_ref[1].astype(f32)
    token_squares = jnp.sum(near * near + far * far, axis=1, keepdims=True)
    half = token_squares.shape[0] // 2
    token_squares = jnp.where(first, token_squares[:half], token_squares[half:])
    squares = jnp.concatenate([squares, token_squares], axis=0) * (1.0 / D)
    parts = three_parts(to_row(squares, 256))
    line = iota((8, 256), 0)
    extra = jnp.where(line == 0, parts[0], jnp.where(line == 1, parts[1], parts[2]))
    extra = jnp.where(line < 3, extra, 0.0).astype(bf16)
    own = (own * gain_ref[...]).astype(bf16)
    other = (other * gain_other_ref[...]).astype(bf16)
    for n in range(out_ref.shape[0]):
        cut = slice(n * 128, (n + 1) * 128)
        part = dot(own, jnp.concatenate([gate_ref[:, cut], up_ref[:, cut]], axis=1)) + dot(
            other, jnp.concatenate([gate_other_ref[:, cut], up_other_ref[:, cut]], axis=1)
        )
        out_ref[n, :slots] = part.astype(bf16)
        out_ref[n, slots : slots + half] = (kept_ref[n] + sent_ref[n].astype(f32)).astype(bf16)
        out_ref[n, slots + half :] = extra


def hidden_kernel(parts_ref, out_ref):
    rows = out_ref.shape[0]
    total = parts_ref[0].astype(f32)
    for n in range(1, parts_ref.shape[0]):
        total = total + parts_ref[n].astype(f32)
    mean = total[rows : rows + 1] + total[rows + 1 : rows + 2] + total[rows + 2 : rows + 3]
    scale = to_column(lax.rsqrt(mean + EPS), rows)
    gate = jnp.where(scale > 0.0, total[:rows, :128] * scale, 0.0)
    up = jnp.where(scale > 0.0, total[:rows, 128:] * scale, 0.0)
    out_ref[...] = (gate / (1.0 + jnp.exp(-gate)) * up).astype(bf16)


def lanes_of(ref, core, lo, hi):
    return jnp.concatenate([ref[n, lo:hi] for n in range(core, ref.shape[0], 2)], axis=1)


def down_kernel(hidden_ref, down_ref, out_ref):
    sent = out_ref.shape[0]
    slots = 3 * sent // 8
    down = down_ref[...]
    rows = jnp.concatenate(
        [dot(lanes_of(hidden_ref, core, 0, slots), down).astype(bf16) for core in range(2)], axis=0
    )
    to, at = iota((sent, 2 * slots), 0), iota((sent, 2 * slots), 1)
    place = (to & 7) * (sent // 8) + (to >> 3)
    out_ref[...] = dot(jnp.where(at == place, 1.0, 0.0).astype(bf16), rows).astype(bf16)


def shared_down_kernel(hidden_ref, down_ref, out_ref):
    rows = hidden_ref.shape[1]
    half = out_ref.shape[0] // 2
    hidden = jnp.concatenate(
        [lanes_of(hidden_ref, core, rows - half, rows) for core in range(2)], axis=0
    )
    out_ref[...] = dot(hidden, down_ref[...])


def combine_kernel(rows_ref, weights_ref, shared_ref, mixed_ref, squares_ref):
    rows = rows_ref[...]
    mixed = shared_ref[...]
    for n in range(3):
        mixed = mixed + dot(weights_ref[n], rows)
    mixed_ref[...] = mixed
    squares = to_row(jnp.sum(mixed * mixed, axis=1, keepdims=True), 128)
    squares_ref[...] = jnp.broadcast_to(squares[None], squares_ref.shape)


def norm_kernel(squares_ref, mixed_ref, gain_ref, out_ref):
    total = jnp.sum(squares_ref[...], axis=0)
    scale = to_column(lax.rsqrt(total / D + EPS), out_ref.shape[0])
    out_ref[...] = (mixed_ref[...] * scale * gain_ref[...]).astype(bf16)


def call(body, out, *operands, flops=0):
    def spec(array):
        return pl.BlockSpec(memory_space=pltpu.SMEM if array.shape == (1,) else pltpu.VMEM)

    outs = out if isinstance(out, tuple) else (out,)
    specs = tuple(pl.BlockSpec(memory_space=pltpu.VMEM) for _ in outs)
    moved = sum(a.size * a.dtype.itemsize for a in (*operands, *outs))
    return pl.pallas_call(
        body,
        out_shape=out,
        in_specs=[spec(a) for a in operands],
        out_specs=specs if isinstance(out, tuple) else specs[0],
        compiler_params=pltpu.CompilerParams(vmem_limit_bytes=24 * MIB),
        cost_estimate=pl.CostEstimate(flops=flops, bytes_accessed=moved, transcendentals=0),
        name=body.__name__,
    )(*operands)


def shape(dims, dtype):
    return jax.ShapeDtypeStruct(dims, dtype)


def per_device(
    tokens,
    norm_gain,
    routes,
    route_weights,
    gate_proj,
    up_proj,
    down_proj,
    shared_gate,
    shared_up,
    shared_down,
    out_gain,
):
    rows, features = tokens.shape
    sources, lines, cores = (lax.axis_size(a) for a in ("ep", "x", "core"))
    sent = sources * 8
    slots = sources * 3
    half = rows // 2
    core = lax.axis_index("core").astype(i32).reshape(1)
    swap = [(0, 1), (1, 0)]
    gain = norm_gain.reshape(1, features)
    gate, up, down = gate_proj[0], up_proj[0], down_proj[0]

    both = lax.all_gather(tokens, "core", axis=0)
    outgoing = call(pack_kernel, shape((sent, features), bf16), core, routes, tokens, both)
    arrived = lax.all_to_all(outgoing.reshape(sources, 8, features), "ep", 0, 0, tiled=True)

    gate_other, up_other = lax.ppermute(gate, "core", swap), lax.ppermute(up, "core", swap)
    gain_other = lax.ppermute(gain, "core", swap)
    kept, given = call(
        shared_up_kernel,
        (shape((lines, half, 256), f32), shape((lines, half, 256), bf16)),
        core,
        tokens,
        gain,
        shared_gate,
        shared_up,
        flops=2 * rows * features * 2048,
    )
    taken = lax.ppermute(given, "core", swap)

    parts = call(
        hidden_parts_kernel,
        shape((lines, slots + half + 8, 256), bf16),
        core,
        arrived.reshape(sent, features),
        both,
        gain,
        gain_other,
        gate,
        up,
        gate_other,
        up_other,
        kept,
        taken,
        flops=4 * slots * features * 2048,
    )
    parts = lax.all_to_all(parts, "x", 0, 0, tiled=True)
    hidden = call(hidden_kernel, shape((slots + half, 128), bf16), parts)
    hidden = lax.all_gather(hidden, ("x", "core"), axis=0)
    leaving = call(
        down_kernel, shape((sent, features), bf16), hidden, down, flops=4 * slots * 1024 * features
    )
    returned = lax.all_to_all(leaving.reshape(sources, 8, features), "ep", 0, 0, tiled=True)
    shared = call(
        shared_down_kernel,
        shape((rows, features), f32),
        hidden,
        shared_down,
        flops=2 * rows * 1024 * features,
    )
    weights = call(weights_kernel, shape((3, rows, sent), bf16), routes, route_weights)
    mixed, squares = call(
        combine_kernel,
        (shape((rows, features), f32), shape((lines * cores, 1, 128), f32)),
        returned.reshape(sent, features),
        weights,
        shared,
    )
    squares = lax.all_to_all(squares, ("x", "core"), 0, 0, tiled=True)
    return call(
        norm_kernel,
        shape((rows, features), bf16),
        squares,
        mixed,
        out_gain.reshape(1, features),
    )


def solution(mesh):
    sources, members = mesh.devices.shape
    inner = Mesh(mesh.devices.reshape(sources, members // 2, 2), ("ep", "x", "core"))
    tp = ("x", "core")
    return jax.shard_map(
        per_device,
        mesh=inner,
        in_specs=(
            P("ep", tp),
            P(tp),
            P("ep", None),
            P("ep", None),
            P("ep", tp, None),
            P("ep", tp, None),
            P("ep", None, tp),
            P(tp, None),
            P(tp, None),
            P(None, tp),
            P(tp),
        ),
        out_specs=P("ep", tp),
        check_vma=False,
    )
```

time: 209 us -> 134 us (0.64)
  waiting for transfers between devices: 82.6 us -> 19.4 us
  blocking collectives: 32 us -> 64.4 us
  local copies, waits for them, and re-layouts: 22.8 us -> 3.25 us
  between operations: 13.6 us -> 0.14 us
  other arithmetic: 6.38 us -> 0 us
  matrix products: 5.62 us -> 0 us
  Pallas kernels: 0 us -> 5.42 us
  starting transfers between devices: 45.6 us -> 40.3 us
    reduce_scatter x1 -> x0, waiting for transfers between devices: 53.6 us -> none  [one_scatter(): lax.psum_scatter(lines, axis, tiled=True).reshape(-1)]
    all_to_all x3 -> x2, starting transfers between devices: 45.5 us -> 17.6 us  [the longest x1 10.5 us: per_device(): lax.all_to_all(outgoing.reshape(sources, 8, features), 'ep', 0, 0, tiled=...]
    all_to_all x1 -> x2, blocking collectives: 13.6 us -> 41.2 us  [the longest x1 28.2 us: per_device(): parts = lax.all_to_all(parts, 'x', 0, 0, tiled=True)]
    ppermute x0 -> x4, starting transfers between devices: none -> 22.7 us  [the longest x1 16.1 us: per_device(): lax.ppermute(gate, 'core', swap)]
    reshape x17 -> x0, local copies, waits for them, and re-layouts: 16.5 us -> none  [the longest x8 9.17 us: split_up(): array.reshape(*lengths[:dim], devices, lengths[dim] // devices, *lengths[...]
    all_to_all x3 -> x2, waiting for transfers between devices: 29 us -> 18.3 us  [the longest x1 12.8 us: per_device(): lax.all_to_all(leaving.reshape(sources, 8, features), 'ep', 0, 0, tiled=T...]
    dot_general x6 -> x0, matrix products: 5.62 us -> none  [the longest x1 2 us: per_device(): jnp.einsum('sjcf,jfd->sjcd', hidden, down_proj, preferred_element_type=jn...]
    pallas_call x0 -> x9, Pallas kernels: none -> 5.42 us  [call(): pl.pallas_call(body, out_shape=out, in_specs=[spec(a) for a in operands],...]
  transfers between devices with their start and end apart: 4 -> 6, of which waited for: 4 -> 3; matrix products, arithmetic and copies ran while one was open for 2% -> 1% of each run, Pallas kernels for 0% -> 1%
where the time goes in v1:
time: 134 us; the launch traced here: 133 us
  blocking collectives  64.4 us (48%)
  starting transfers between devices  40.3 us (30%)
  waiting for transfers between devices  19.4 us (14%)
  Pallas kernels  5.42 us (4%)
  local copies, waits for them, and re-layouts  3.25 us (2%)
    all_to_all x1, blocking collectives, per_device(): parts = lax.all_to_all(parts, 'x', 0, 0, tiled=True)  28.2 us
    all_gather x1, blocking collectives, per_device(): hidden = lax.all_gather(hidden, ('x', 'core'), axis=0)  21.2 us
    ppermute x1, starting transfers between devices, per_device(): lax.ppermute(gate, 'core', swap)  16.1 us
    all_to_all x1, blocking collectives, per_device(): squares = lax.all_to_all(squares, ('x', 'core'), 0, 0, tiled=True)  13 us
    all_to_all x1, waiting for transfers between devices, per_device(): lax.all_to_all(leaving.reshape(sources, 8, features), 'ep', 0, 0, tiled=T...  12.8 us
    all_to_all x1, starting transfers between devices, per_device(): lax.all_to_all(outgoing.reshape(sources, 8, features), 'ep', 0, 0, tiled=...  10.5 us
    all_to_all x1, starting transfers between devices, per_device(): lax.all_to_all(leaving.reshape(sources, 8, features), 'ep', 0, 0, tiled=T...  7.12 us
    all_to_all x1, waiting for transfers between devices, per_device(): lax.all_to_all(outgoing.reshape(sources, 8, features), 'ep', 0, 0, tiled=...  5.45 us
  transfers between devices with their start and end apart: 6, of which 3 were waited for; matrix products, arithmetic and copies ran while one was open for 1% of the time, Pallas kernels for 1%

profile of v1, /device:TPU:1, one launch (start us, length us, event | category | flops | bytes accessed | tf_op | source)
XLA Modules:
  0.0 132.9 jit_solution(15947755027679063849)
XLA Ops:
  0.0 0.0 copy-start.6
  0.0 0.0 copy-start.3
  0.0 16.1 %collective-permute-start.1 = (bf16[256,1024]{1,0:T(8,128)(2,1)}, bf16[256,1024]{1,0:T(8,128)(2,1)S(1)}, u32[]{:S(2)}, u32[]{:S(2)}) collective-permute-start(bf16[256,1024]{1,0:T(8,128)(2,1)} %bitcast.16), channel_id=1, source_target_pairs={{0,1},{1,0},{2,3},{3,2},{4,5},{5,4},{6,7},{7,6},{8,9},{9,8},{10,11... | collective-permute-start | bytes 1572872 | tf_op jit(solution)/shard_map/ppermute | solution.py:243
  16.2 1.9 %collective-permute-start.2 = (bf16[256,1024]{1,0:T(8,128)(2,1)}, bf16[256,1024]{1,0:T(8,128)(2,1)S(1)}, u32[]{:S(2)}, u32[]{:S(2)}) collective-permute-start(bf16[256,1024]{1,0:T(8,128)(2,1)} %bitcast.18), channel_id=1, source_target_pairs={{0,1},{1,0},{2,3},{3,2},{4,5},{5,4},{6,7},{7,6},{8,9},{9,8},{10,11... | collective-permute-start | bytes 1572872 | tf_op jit(solution)/shard_map/ppermute | solution.py:243
  18.1 0.8 copy.12.routes_ref
  18.9 0.0 copy-done.6
  18.9 2.0 %all-gather = bf16[64,256]{1,0:T(8,128)(2,1)S(1)} all-gather(bf16[32,256]{1,0:T(8,128)(2,1)S(1)} %copy-done.6), channel_id=2, replica_groups=mesh['ep'=64,'x'=8,'core'=2] {'core'}, dimensions={0}, use_global_device_ids=true | all-gather | bytes 49152 | tf_op jit(solution)/shard_map/all_gather | solution.py:239
  20.8 1.2 pack_kernel.1
  22.0 10.5 %all-to-all-start = ((bf16[64,8,256]{2,1,0:T(8,128)(2,1)}), bf16[64,8,256]{2,1,0:T(8,128)(2,1)S(1)}, u32[]{:S(2)}, u32[]{:S(2)}) async-start(bf16[64,8,256]{2,1,0:T(8,128)(2,1)} %bitcast.2), calls=%async_computation | async-start | bytes 524288 | tf_op jit(solution)/shard_map/all_to_all | solution.py:241
  32.6 0.0 copy-start.7
  32.6 0.0 copy-done.3
  32.6 0.7 copy-done.7
  33.2 0.0 copy-start.4
  33.2 1.0 copy-done.4
  34.3 0.0 copy-start
  34.3 0.0 copy-start.1
  34.3 0.3 shared_up_kernel.1
  34.6 2.7 %collective-permute-start.3 = (bf16[8,16,256]{2,1,0:T(8,128)(2,1)S(1)}, bf16[8,16,256]{2,1,0:T(8,128)(2,1)S(1)}, u32[]{:S(2)}, u32[]{:S(2)}) collective-permute-start(bf16[8,16,256]{2,1,0:T(8,128)(2,1)S(1)} %get-tuple-element.10), channel_id=1, source_target_pairs={{0,1},{1,0},{2,3},{3,2},{4,5},{5,4},{6,7},{7,6},{8,9},{9,8},{10,11... | collective-permute-start | bytes 196616 | tf_op jit(solution)/shard_map/ppermute | solution.py:255
  37.2 1.9 %collective-permute-start = (f32[1,256]{1,0:T(1,128)S(1)}, f32[1,256]{1,0:T(1,128)S(1)}, u32[]{:S(2)}, u32[]{:S(2)}) collective-permute-start(f32[1,256]{1,0:T(1,128)S(1)} %bitcast.24), channel_id=1, source_target_pairs={{0,1},{1,0},{2,3},{3,2},{4,5},{5,4},{6,7},{7,6},{8,9},{9,8},{10,11... | collective-permute-start | bytes 3080 | tf_op jit(solution)/shard_map/ppermute | solution.py:244
  39.2 1.1 collective-permute-done.gain_other_ref
  40.3 0.0 collective-permute-done.3.sent_ref
  40.3 5.4 %all-to-all-done = bf16[64,8,256]{2,1,0:T(8,128)(2,1)S(1)} async-done(((bf16[64,8,256]{2,1,0:T(8,128)(2,1)}), bf16[64,8,256]{2,1,0:T(8,128)(2,1)S(1)}, u32[]{:S(2)}, u32[]{:S(2)}) %all-to-all-start) | async-done | bytes 262176 | tf_op jit(solution)/shard_map/all_to_all | solution.py:241
  45.8 0.0 collective-permute-done.1.gate_other_ref
  45.8 0.0 collective-permute-done.2.up_other_ref
  45.8 0.0 copy-done
  45.8 0.0 copy-done.1
  45.8 0.9 hidden_parts_kernel.1
  46.7 28.2 %all_to_all.20.parts_ref = bf16[8,216,256]{2,1,0:T(8,128)(2,1)S(1)} all-to-all(bf16[8,216,256]{2,1,0:T(8,128)(2,1)S(1)} %hidden_parts_kernel.1), channel_id=1, replica_groups=mesh['ep'=64,'x'=8,'core'=2] {'x'}, dimensions={0} | all-to-all | bytes 1769472 | tf_op jit(solution)/shard_map/all_to_all | solution.py:273
  74.9 0.2 hidden_kernel.1
  75.1 0.0 copy-start.2
  75.1 21.2 %all-gather.1 = bf16[3328,128]{1,0:T(8,128)(2,1)S(1)} all-gather(bf16[208,128]{1,0:T(8,128)(2,1)S(1)} %hidden_kernel.1), channel_id=3, replica_groups=mesh['ep'=64,'x'=8,'core'=2] {'x','core'}, dimensions={0}, use_global_device_ids=true | all-gather | bytes 905216 | tf_op jit(solution)/shard_map/all_gather | solution.py:275
  96.3 0.0 copy-done.2
  96.3 0.0 copy-start.9
  96.3 1.4 %down_kernel.1 = bf16[512,256]{1,0:T(8,128)(2,1)} custom-call(bf16[16,208,128]{2,1,0:T(8,128)(2,1)S(1)} %bitcast.12, bf16[1024,256]{1,0:T(8,128)(2,1)S(1)} %bitcast.20), custom_call_target="tpu_custom_call" | custom-call | flops 201326592 | bytes 1638400 | tf_op jit(solution)/shard_map/down_kernel/pallas_call | solution.py:201
  97.7 0.0 copy-start.5
  97.7 7.1 %all-to-all-start.2 = ((bf16[64,8,256]{2,1,0:T(8,128)(2,1)}), bf16[64,8,256]{2,1,0:T(8,128)(2,1)S(1)}, u32[]{:S(2)}, u32[]{:S(2)}) async-start(bf16[64,8,256]{2,1,0:T(8,128)(2,1)} %bitcast.9), calls=%async_computation.2 | async-start | bytes 524288 | tf_op jit(solution)/shard_map/all_to_all | solution.py:279
  104.8 0.0 copy-done.9
  104.8 0.1 copy.14.weights_ref
  104.9 0.3 weights_kernel.1.weights_ref
  105.2 0.0 copy-done.5
  105.2 0.2 shared_down_kernel.1.shared_ref
  105.4 12.8 %all-to-all-done.2 = bf16[64,8,256]{2,1,0:T(8,128)(2,1)S(1)} async-done(((bf16[64,8,256]{2,1,0:T(8,128)(2,1)}), bf16[64,8,256]{2,1,0:T(8,128)(2,1)S(1)}, u32[]{:S(2)}, u32[]{:S(2)}) %all-to-all-start.2) | async-done | bytes 262176 | tf_op jit(solution)/shard_map/all_to_all | solution.py:279
  118.2 0.3 combine_kernel.1
  118.6 13.0 %all_to_all.21.squares_ref = f32[16,1,128]{2,1,0:T(1,128)S(1)} all-to-all(f32[16,1,128]{2,1,0:T(1,128)S(1)} %get-tuple-element.11), channel_id=1, replica_groups=mesh['ep'=64,'x'=8,'core'=2] {'x','core'}, dimensions={0} | all-to-all | bytes 16384 | tf_op jit(solution)/shard_map/all_to_all | solution.py:295
  131.5 0.0 copy-start.8
  131.5 0.7 copy-done.8
  132.2 0.7 norm_kernel.1
Async XLA Ops:
  0.0 18.9 %copy-start.6 = (bf16[32,256]{1,0:T(8,128)(2,1)S(1)}, bf16[32,256]{1,0:T(8,128)(2,1)}, u32[]{:S(2)}) copy-start(bf16[32,256]{1,0:T(8,128)(2,1)} %own_ref.3) | copy-start | bytes 49156
  0.0 32.6 %copy-start.3 = (bf16[256,1024]{1,0:T(8,128)(2,1)S(1)}, bf16[256,1024]{1,0:T(8,128)(2,1)}, u32[]{:S(2)}) copy-start(bf16[256,1024]{1,0:T(8,128)(2,1)} %gate_ref.1) | copy-start | bytes 1572868
  0.0 45.7 %collective-permute-start.1 = (bf16[256,1024]{1,0:T(8,128)(2,1)}, bf16[256,1024]{1,0:T(8,128)(2,1)S(1)}, u32[]{:S(2)}, u32[]{:S(2)}) collective-permute-start(bf16[256,1024]{1,0:T(8,128)(2,1)} %bitcast.16), channel_id=1, source_target_pairs={{0,1},{1,0},{2,3},{3,2},{4,5},{5,4},{6,7},{7,6},{8,9},{9,8},{10,11... | collective-permute-start | bytes 1572872 | tf_op jit(solution)/shard_map/ppermute | solution.py:243
  16.2 29.6 %collective-permute-start.2 = (bf16[256,1024]{1,0:T(8,128)(2,1)}, bf16[256,1024]{1,0:T(8,128)(2,1)S(1)}, u32[]{:S(2)}, u32[]{:S(2)}) collective-permute-start(bf16[256,1024]{1,0:T(8,128)(2,1)} %bitcast.18), channel_id=1, source_target_pairs={{0,1},{1,0},{2,3},{3,2},{4,5},{5,4},{6,7},{7,6},{8,9},{9,8},{10,11... | collective-permute-start | bytes 1572872 | tf_op jit(solution)/shard_map/ppermute | solution.py:243
  22.0 23.7 %all-to-all-start = ((bf16[64,8,256]{2,1,0:T(8,128)(2,1)}), bf16[64,8,256]{2,1,0:T(8,128)(2,1)S(1)}, u32[]{:S(2)}, u32[]{:S(2)}) async-start(bf16[64,8,256]{2,1,0:T(8,128)(2,1)} %bitcast.2), calls=%async_computation | async-start | bytes 524288 | tf_op jit(solution)/shard_map/all_to_all | solution.py:241
  32.6 0.7 copy-start.7
  33.2 1.0 copy-start.4
  34.3 11.5 %copy-start = (bf16[1,256,1024]{2,1,0:T(8,128)(2,1)S(1)}, bf16[1,256,1024]{2,1,0:T(8,128)(2,1)}, u32[]{:S(2)}) copy-start(bf16[1,256,1024]{2,1,0:T(8,128)(2,1)} %param.15) | copy-start | bytes 1572868
  34.3 11.5 %copy-start.1 = (bf16[1,256,1024]{2,1,0:T(8,128)(2,1)S(1)}, bf16[1,256,1024]{2,1,0:T(8,128)(2,1)}, u32[]{:S(2)}) copy-start(bf16[1,256,1024]{2,1,0:T(8,128)(2,1)} %param.16) | copy-start | bytes 1572868
  34.6 5.7 %collective-permute-start.3 = (bf16[8,16,256]{2,1,0:T(8,128)(2,1)S(1)}, bf16[8,16,256]{2,1,0:T(8,128)(2,1)S(1)}, u32[]{:S(2)}, u32[]{:S(2)}) collective-permute-start(bf16[8,16,256]{2,1,0:T(8,128)(2,1)S(1)} %get-tuple-element.10), channel_id=1, source_target_pairs={{0,1},{1,0},{2,3},{3,2},{4,5},{5,4},{6,7},{7,6},{8,9},{9,8},{10,11... | collective-permute-start | bytes 196616 | tf_op jit(solution)/shard_map/ppermute | solution.py:255
  37.2 3.1 %collective-permute-start = (f32[1,256]{1,0:T(1,128)S(1)}, f32[1,256]{1,0:T(1,128)S(1)}, u32[]{:S(2)}, u32[]{:S(2)}) collective-permute-start(f32[1,256]{1,0:T(1,128)S(1)} %bitcast.24), channel_id=1, source_target_pairs={{0,1},{1,0},{2,3},{3,2},{4,5},{5,4},{6,7},{7,6},{8,9},{9,8},{10,11... | collective-permute-start | bytes 3080 | tf_op jit(solution)/shard_map/ppermute | solution.py:244
  75.1 21.2 %copy-start.2 = (bf16[1,1024,256]{2,1,0:T(8,128)(2,1)S(1)}, bf16[1,1024,256]{2,1,0:T(8,128)(2,1)}, u32[]{:S(2)}) copy-start(bf16[1,1024,256]{2,1,0:T(8,128)(2,1)} %param.17) | copy-start | bytes 1572868
  96.3 8.5 %copy-start.9 = (f32[32,8]{0,1:T(8,128)S(1)}, f32[32,8]{0,1:T(8,128)}, u32[]{:S(2)}) copy-start(f32[32,8]{0,1:T(8,128)} %param.14) | copy-start | bytes 3076
  97.7 7.5 %copy-start.5 = (bf16[1024,256]{1,0:T(8,128)(2,1)S(1)}, bf16[1024,256]{1,0:T(8,128)(2,1)}, u32[]{:S(2)}) copy-start(bf16[1024,256]{1,0:T(8,128)(2,1)} %down_ref.1) | copy-start | bytes 1572868
  97.7 20.6 %all-to-all-start.2 = ((bf16[64,8,256]{2,1,0:T(8,128)(2,1)}), bf16[64,8,256]{2,1,0:T(8,128)(2,1)S(1)}, u32[]{:S(2)}, u32[]{:S(2)}) async-start(bf16[64,8,256]{2,1,0:T(8,128)(2,1)} %bitcast.9), calls=%async_computation.2 | async-start | bytes 524288 | tf_op jit(solution)/shard_map/all_to_all | solution.py:279
  131.5 0.7 copy-start.8

commit v2 on v1

--- a/solution.py
+++ b/solution.py
@@ -4,6 +4,7 @@
 from jax.experimental import pallas as pl
 from jax.experimental.pallas import tpu as pltpu
 from jax.sharding import Mesh, PartitionSpec as P
+
 
 D = 4096
 EPS = 1e-06
@@ -49,10 +50,10 @@
     return named, rank.astype(i32)
 
 
-def pack_kernel(core_ref, routes_ref, own_ref, both_ref, out_ref):
+def pack_kernel(core_ref, routes_ref, both_ref, out_ref):
     core = core_ref[0]
     lanes = out_ref.shape[0]
-    named, rank = named_slots(routes_ref[...], lanes)
+    named, rank = named_slots(routes_ref[...].T, lanes)
     lane = iota(named.shape, 1)
     slot = lane & 3
     chosen = named & (rank == 3 * core + slot) & (slot < 3)
@@ -64,34 +65,53 @@
         ],
         axis=0,
     )
-    rows = jnp.concatenate([own_ref[...], both_ref[1 - core]], axis=0)
+    rows = jnp.concatenate([both_ref[core], both_ref[1 - core]], axis=0)
     out_ref[...] = lax.dot_general(
         picks, rows, (((0,), (0,)), ((), ())), preferred_element_type=f32
     ).astype(bf16)
 
 
-def weights_kernel(routes_ref, weights_ref, out_ref):
-    routes = routes_ref[...]
+def combine_weights(routes_ref, weights_ref, out_ref):
+    routes, given = routes_ref[...].T, weights_ref[...].T
     lanes = out_ref.shape[2]
     named, rank = named_slots(routes, lanes)
     lane = iota(named.shape, 1)
     weight = jnp.zeros(named.shape, f32)
     for k in range(routes.shape[1]):
-        weight = jnp.where(routes[:, k : k + 1] == lane >> 3, weights_ref[:, k : k + 1], weight)
+        weight = jnp.where(routes[:, k : k + 1] == lane >> 3, given[:, k : k + 1], weight)
     weight = jnp.where(named & (rank == (lane & 7)), weight, 0.0)
     for n, part in enumerate(three_parts(weight)):
         out_ref[n] = part.astype(bf16)
 
 
-def shared_up_kernel(core_ref, own_ref, gain_ref, gate_ref, up_ref, keep_ref, send_ref):
+def shared_up_kernel(
+    core_ref,
+    both_ref,
+    gain_ref,
+    gate_ref,
+    up_ref,
+    routes_ref,
+    weights_ref,
+    out_gain_ref,
+    keep_ref,
+    send_ref,
+    combine_ref,
+    later_gain_ref,
+):
+    later_gain_ref[...] = out_gain_ref[...]
+    combine_weights(routes_ref, weights_ref, combine_ref)
     first = core_ref[0] == 0
-    rows = (own_ref[...].astype(f32) * gain_ref[...]).astype(bf16)
+    rows = (both_ref[core_ref[0]].astype(f32) * gain_ref[...]).astype(bf16)
     half = rows.shape[0] // 2
     for n in range(keep_ref.shape[0]):
         cut = slice(n * 128, (n + 1) * 128)
         part = dot(rows, jnp.concatenate([gate_ref[:, cut], up_ref[:, cut]], axis=1))
         keep_ref[n] = jnp.where(first, part[:half], part[half:])
         send_ref[n] = jnp.where(first, part[half:], part[:half]).astype(bf16)
+    parts = three_parts(gain_ref[...])
+    line = iota(send_ref.shape[1:], 0)
+    gain = jnp.where(line == 0, parts[0], jnp.where(line == 1, parts[1], parts[2]))
+    send_ref[keep_ref.shape[0]] = jnp.where(line < 3, gain, 0.0).astype(bf16)
 
 
 def hidden_parts_kernel(
@@ -99,7 +119,6 @@
     rows_ref,
     both_ref,
     gain_ref,
-    gain_other_ref,
     gate_ref,
     up_ref,
     gate_other_ref,
@@ -127,7 +146,9 @@
     extra = jnp.where(line == 0, parts[0], jnp.where(line == 1, parts[1], parts[2]))
     extra = jnp.where(line < 3, extra, 0.0).astype(bf16)
     own = (own * gain_ref[...]).astype(bf16)
-    other = (other * gain_other_ref[...]).astype(bf16)
+    swapped = sent_ref[out_ref.shape[0]].astype(f32)
+    gain_other = swapped[0:1] + swapped[1:2] + swapped[2:3]
+    other = (other * gain_other).astype(bf16)
     for n in range(out_ref.shape[0]):
         cut = slice(n * 128, (n + 1) * 128)
         part = dot(own, jnp.concatenate([gate_ref[:, cut], up_ref[:, cut]], axis=1)) + dot(
@@ -154,7 +175,7 @@
     return jnp.concatenate([ref[n, lo:hi] for n in range(core, ref.shape[0], 2)], axis=1)
 
 
-def down_kernel(hidden_ref, down_ref, out_ref):
+def down_kernel(hidden_ref, down_ref, shared_down_ref, out_ref, shared_ref):
     sent = out_ref.shape[0]
     slots = 3 * sent // 8
     down = down_ref[...]
@@ -165,30 +186,27 @@
     place = (to & 7) * (sent // 8) + (to >> 3)
     out_ref[...] = dot(jnp.where(at == place, 1.0, 0.0).astype(bf16), rows).astype(bf16)
 
-
-def shared_down_kernel(hidden_ref, down_ref, out_ref):
-    rows = hidden_ref.shape[1]
-    half = out_ref.shape[0] // 2
+    end = hidden_ref.shape[1]
     hidden = jnp.concatenate(
-        [lanes_of(hidden_ref, core, rows - half, rows) for core in range(2)], axis=0
-    )
-    out_ref[...] = dot(hidden, down_ref[...])
-
-
-def combine_kernel(rows_ref, weights_ref, shared_ref, mixed_ref, squares_ref):
+        [lanes_of(hidden_ref, core, slots, end) for core in range(2)], axis=0
+    )
+    shared_ref[...] = dot(hidden, shared_down_ref[...])
+
+
+def combine_kernel(rows_ref, weights_ref, shared_ref, gain_ref, mixed_ref, squares_ref):
     rows = rows_ref[...]
     mixed = shared_ref[...]
     for n in range(3):
         mixed = mixed + dot(weights_ref[n], rows)
-    mixed_ref[...] = mixed
+    mixed_ref[...] = mixed * gain_ref[...]
     squares = to_row(jnp.sum(mixed * mixed, axis=1, keepdims=True), 128)
     squares_ref[...] = jnp.broadcast_to(squares[None], squares_ref.shape)
 
 
-def norm_kernel(squares_ref, mixed_ref, gain_ref, out_ref):
+def norm_kernel(squares_ref, mixed_ref, out_ref):
     total = jnp.sum(squares_ref[...], axis=0)
     scale = to_column(lax.rsqrt(total / D + EPS), out_ref.shape[0])
-    out_ref[...] = (mixed_ref[...] * scale * gain_ref[...]).astype(bf16)
+    out_ref[...] = (mixed_ref[...] * scale).astype(bf16)
 
 
 def call(body, out, *operands, flops=0):
@@ -205,7 +223,6 @@
         out_specs=specs if isinstance(out, tuple) else specs[0],
         compiler_params=pltpu.CompilerParams(vmem_limit_bytes=24 * MIB),
         cost_estimate=pl.CostEstimate(flops=flops, bytes_accessed=moved, transcendentals=0),
-        name=body.__name__,
     )(*operands)
 
 
@@ -236,20 +253,30 @@
     gain = norm_gain.reshape(1, features)
     gate, up, down = gate_proj[0], up_proj[0], down_proj[0]
 
+    routes, route_weights = routes.T, route_weights.T
     both = lax.all_gather(tokens, "core", axis=0)
-    outgoing = call(pack_kernel, shape((sent, features), bf16), core, routes, tokens, both)
-    arrived = lax.all_to_all(outgoing.reshape(sources, 8, features), "ep", 0, 0, tiled=True)
-
-    gate_other, up_other = lax.ppermute(gate, "core", swap), lax.ppermute(up, "core", swap)
-    gain_other = lax.ppermute(gain, "core", swap)
-    kept, given = call(
+    outgoing = call(pack_kernel, shape((sent, features), bf16), core, routes, both)
+    arrived = lax.all_to_all(
+        outgoing.reshape(sources, 8, features), "ep", 0, 0, tiled=True
+    )
+    gate_other = lax.ppermute(gate, "core", swap)
+    up_other = lax.ppermute(up, "core", swap)
+    kept, given, weights, later_gain = call(
         shared_up_kernel,
-        (shape((lines, half, 256), f32), shape((lines, half, 256), bf16)),
+        (
+            shape((lines, half, 256), f32),
+            shape((lines + 1, half, 256), bf16),
+            shape((3, rows, sent), bf16),
+            shape((1, features), f32),
+        ),
         core,
-        tokens,
+        both,
         gain,
         shared_gate,
         shared_up,
+        routes,
+        route_weights,
+        out_gain.reshape(1, features),
         flops=2 * rows * features * 2048,
     )
     taken = lax.ppermute(given, "core", swap)
@@ -261,7 +288,6 @@
         arrived.reshape(sent, features),
         both,
         gain,
-        gain_other,
         gate,
         up,
         gate_other,
@@ -273,33 +299,25 @@
     parts = lax.all_to_all(parts, "x", 0, 0, tiled=True)
     hidden = call(hidden_kernel, shape((slots + half, 128), bf16), parts)
     hidden = lax.all_gather(hidden, ("x", "core"), axis=0)
-    leaving = call(
-        down_kernel, shape((sent, features), bf16), hidden, down, flops=4 * slots * 1024 * features
+    leaving, shared = call(
+        down_kernel,
+        (shape((sent, features), bf16), shape((rows, features), f32)),
+        hidden,
+        down,
+        shared_down,
+        flops=4 * slots * 1024 * features,
     )
     returned = lax.all_to_all(leaving.reshape(sources, 8, features), "ep", 0, 0, tiled=True)
-    shared = call(
-        shared_down_kernel,
-        shape((rows, features), f32),
-        hidden,
-        shared_down,
-        flops=2 * rows * 1024 * features,
-    )
-    weights = call(weights_kernel, shape((3, rows, sent), bf16), routes, route_weights)
     mixed, squares = call(
         combine_kernel,
         (shape((rows, features), f32), shape((lines * cores, 1, 128), f32)),
         returned.reshape(sent, features),
         weights,
         shared,
+        later_gain,
     )
     squares = lax.all_to_all(squares, ("x", "core"), 0, 0, tiled=True)
-    return call(
-        norm_kernel,
-        shape((rows, features), bf16),
-        squares,
-        mixed,
-        out_gain.reshape(1, features),
-    )
+    return call(norm_kernel, shape((rows, features), bf16), squares, mixed)
 
 
 def solution(mesh):

time: 134 us -> 131 us (0.978)
  blocking collectives: 64.4 us -> 83.3 us
  waiting for transfers between devices: 19.4 us -> 8.37 us
  starting transfers between devices: 40.3 us -> 31.3 us
    all_to_all x0 -> x1, blocking collectives: none -> 18.5 us  [per_device(): lax.all_to_all(leaving.reshape(sources, 8, features), 'ep', 0, 0, tiled=T...]
    all_to_all x1 -> x0, waiting for transfers between devices: 12.8 us -> none  [per_device(): lax.all_to_all(leaving.reshape(sources, 8, features), 'ep', 0, 0, tiled=T...]
    all_to_all x1 -> x0, starting transfers between devices: 7.12 us -> none  [per_device(): lax.all_to_all(leaving.reshape(sources, 8, features), 'ep', 0, 0, tiled=T...]
    all_to_all x1, waiting for transfers between devices: 5.45 us -> 7.47 us  [per_device(): lax.all_to_all(outgoing.reshape(sources, 8, features), 'ep', 0, 0, tiled=...]
    ppermute x3 -> x2, starting transfers between devices: 20 us -> 18.1 us  [the longest x1 16.1 us: per_device(): gate_other = lax.ppermute(gate, 'core', swap)]
    pallas_call x9 -> x7, Pallas kernels: 5.42 us -> 4.66 us  [call(): pl.pallas_call(body, out_shape=out, in_specs=[spec(a) for a in operands],...]
  transfers between devices with their start and end apart: 6 -> 4, of which waited for: 3 -> 2; matrix products, arithmetic and copies ran while one was open for 1% -> 0% of each run, Pallas kernels for 1% -> 1%
where the time goes in v2:
time: 131 us; the launch traced here: 130 us
  blocking collectives  83.3 us (64%)
  starting transfers between devices  31.3 us (24%)
  waiting for transfers between devices  8.37 us (6%)
  Pallas kernels  4.66 us (4%)
  local copies, waits for them, and re-layouts  2.41 us (2%)
    all_to_all x1, blocking collectives, per_device(): parts = lax.all_to_all(parts, 'x', 0, 0, tiled=True)  28.2 us
    all_gather x1, blocking collectives, per_device(): hidden = lax.all_gather(hidden, ('x', 'core'), axis=0)  21.3 us
    all_to_all x1, blocking collectives, per_device(): lax.all_to_all(leaving.reshape(sources, 8, features), 'ep', 0, 0, tiled=T...  18.5 us
    ppermute x1, starting transfers between devices, per_device(): gate_other = lax.ppermute(gate, 'core', swap)  16.1 us
    all_to_all x1, blocking collectives, per_device(): squares = lax.all_to_all(squares, ('x', 'core'), 0, 0, tiled=True)  13.1 us
    all_to_all x1, starting transfers between devices, per_device(): lax.all_to_all(outgoing.reshape(sources, 8, features), 'ep', 0, 0, tiled=...  10.6 us
    all_to_all x1, waiting for transfers between devices, per_device(): lax.all_to_all(outgoing.reshape(sources, 8, features), 'ep', 0, 0, tiled=...  7.47 us
    pallas_call x7, Pallas kernels, call(): pl.pallas_call(body, out_shape=out, in_specs=[spec(a) for a in operands],...  4.66 us
  transfers between devices with their start and end apart: 4, of which 2 were waited for; matrix products, arithmetic and copies ran while one was open for 0% of the time, Pallas kernels for 1%

profile of v2, /device:TPU:1, one launch (start us, length us, event | category | flops | bytes accessed | tf_op | source)
XLA Modules:
  0.0 130.1 jit_solution(9156781063649827466)
XLA Ops:
  0.0 0.0 copy-start
  0.0 16.1 %collective-permute-start = (bf16[256,1024]{1,0:T(8,128)(2,1)}, bf16[256,1024]{1,0:T(8,128)(2,1)S(1)}, u32[]{:S(2)}, u32[]{:S(2)}) collective-permute-start(bf16[256,1024]{1,0:T(8,128)(2,1)} %bitcast.20), channel_id=1, source_target_pairs={{0,1},{1,0},{2,3},{3,2},{4,5},{5,4},{6,7},{7,6},{8,9},{9,8},{10,11... | collective-permute-start | bytes 1572872 | tf_op jit(solution)/shard_map/ppermute | solution.py:262
  16.2 1.9 %collective-permute-start.1 = (bf16[256,1024]{1,0:T(8,128)(2,1)}, bf16[256,1024]{1,0:T(8,128)(2,1)S(1)}, u32[]{:S(2)}, u32[]{:S(2)}) collective-permute-start(bf16[256,1024]{1,0:T(8,128)(2,1)} %bitcast.22), channel_id=1, source_target_pairs={{0,1},{1,0},{2,3},{3,2},{4,5},{5,4},{6,7},{7,6},{8,9},{9,8},{10,11... | collective-permute-start | bytes 1572872 | tf_op jit(solution)/shard_map/ppermute | solution.py:263
  18.1 2.2 %all-gather = bf16[64,256]{1,0:T(8,128)(2,1)S(1)} all-gather(bf16[32,256]{1,0:T(8,128)(2,1)} %param.11), channel_id=2, replica_groups=mesh['ep'=64,'x'=8,'core'=2] {'core'}, dimensions={0}, use_global_device_ids=true | all-gather | bytes 49152 | tf_op jit(solution)/shard_map/all_gather | solution.py:257
  20.3 0.0 copy-start.6
  20.3 0.7 copy-done.6
  21.0 1.3 shard_map.109
  22.3 0.0 copy-start.8
  22.3 0.0 copy-start.10
  22.3 10.6 %all-to-all-start = ((bf16[64,8,256]{2,1,0:T(8,128)(2,1)}), bf16[64,8,256]{2,1,0:T(8,128)(2,1)S(1)}, u32[]{:S(2)}, u32[]{:S(2)}) async-start(bf16[64,8,256]{2,1,0:T(8,128)(2,1)} %bitcast.3), calls=%async_computation | async-start | bytes 524288 | tf_op jit(solution)/shard_map/all_to_all | solution.py:259
  32.9 0.0 copy-start.7
  32.9 0.0 copy-start.9
  32.9 0.0 copy-done
  33.0 0.0 copy-done.8
  33.0 0.0 copy-done.10
  33.0 0.6 copy-done.7
  33.6 0.0 copy-done.9
  33.6 0.0 copy-start.1
  33.6 1.0 copy-done.1
  34.7 0.0 copy-start.2
  34.7 0.0 copy-start.3
  34.7 0.5 shard_map.110
  35.2 2.5 %collective-permute-start.2 = (bf16[9,16,256]{2,1,0:T(8,128)(2,1)S(1)}, bf16[9,16,256]{2,1,0:T(8,128)(2,1)S(1)}, u32[]{:S(2)}, u32[]{:S(2)}) collective-permute-start(bf16[9,16,256]{2,1,0:T(8,128)(2,1)S(1)} %get-tuple-element.14), channel_id=1, source_target_pairs={{0,1},{1,0},{2,3},{3,2},{4,5},{5,4},{6,7},{7,6},{8,9},{9,8},{10,11... | collective-permute-start | bytes 221192 | tf_op jit(solution)/shard_map/ppermute | solution.py:282
  37.7 0.9 collective-permute-done.2.sent_ref
  38.6 7.5 %all-to-all-done = bf16[64,8,256]{2,1,0:T(8,128)(2,1)S(1)} async-done(((bf16[64,8,256]{2,1,0:T(8,128)(2,1)}), bf16[64,8,256]{2,1,0:T(8,128)(2,1)S(1)}, u32[]{:S(2)}, u32[]{:S(2)}) %all-to-all-start) | async-done | bytes 262176 | tf_op jit(solution)/shard_map/all_to_all | solution.py:259
  46.1 0.0 collective-permute-done.gate_other_ref
  46.1 0.0 collective-permute-done.1.up_other_ref
  46.1 0.0 copy-done.2
  46.1 0.0 copy-done.3
  46.1 0.9 shard_map.111
  47.0 28.2 %all_to_all.20.parts_ref = bf16[8,216,256]{2,1,0:T(8,128)(2,1)S(1)} all-to-all(bf16[8,216,256]{2,1,0:T(8,128)(2,1)S(1)} %shard_map.111), channel_id=1, replica_groups=mesh['ep'=64,'x'=8,'core'=2] {'x'}, dimensions={0} | all-to-all | bytes 1769472 | tf_op jit(solution)/shard_map/all_to_all | solution.py:299
  75.2 0.0 copy-start.5
  75.2 0.2 shard_map.112
  75.4 0.0 copy-start.4
  75.4 21.3 %all-gather.1 = bf16[3328,128]{1,0:T(8,128)(2,1)S(1)} all-gather(bf16[208,128]{1,0:T(8,128)(2,1)S(1)} %shard_map.112), channel_id=3, replica_groups=mesh['ep'=64,'x'=8,'core'=2] {'x','core'}, dimensions={0}, use_global_device_ids=true | all-gather | bytes 905216 | tf_op jit(solution)/shard_map/all_gather | solution.py:301
  96.7 0.0 copy-done.5
  96.7 0.0 copy-done.4
  96.7 0.7 shard_map.113
  97.4 18.5 %all_to_all.21 = bf16[64,8,256]{2,1,0:T(8,128)(2,1)S(1)} all-to-all(bf16[64,8,256]{2,1,0:T(8,128)(2,1)S(1)} %bitcast.25), channel_id=1, replica_groups=mesh['ep'=64,'x'=8,'core'=2] {'ep'}, dimensions={0} | all-to-all | bytes 524288 | tf_op jit(solution)/shard_map/all_to_all | solution.py:310
  115.9 0.3 shard_map.114
  116.3 13.1 %all_to_all.22.squares_ref = f32[16,1,128]{2,1,0:T(1,128)S(1)} all-to-all(f32[16,1,128]{2,1,0:T(1,128)S(1)} %get-tuple-element.19), channel_id=1, replica_groups=mesh['ep'=64,'x'=8,'core'=2] {'x','core'}, dimensions={0} | all-to-all | bytes 16384 | tf_op jit(solution)/shard_map/all_to_all | solution.py:319
  129.4 0.7 shard_map.115
Async XLA Ops:
  0.0 32.9 %copy-start = (bf16[256,1024]{1,0:T(8,128)(2,1)S(1)}, bf16[256,1024]{1,0:T(8,128)(2,1)}, u32[]{:S(2)}) copy-start(bf16[256,1024]{1,0:T(8,128)(2,1)} %gate_ref.1) | copy-start | bytes 1572868
  0.0 46.1 %collective-permute-start = (bf16[256,1024]{1,0:T(8,128)(2,1)}, bf16[256,1024]{1,0:T(8,128)(2,1)S(1)}, u32[]{:S(2)}, u32[]{:S(2)}) collective-permute-start(bf16[256,1024]{1,0:T(8,128)(2,1)} %bitcast.20), channel_id=1, source_target_pairs={{0,1},{1,0},{2,3},{3,2},{4,5},{5,4},{6,7},{7,6},{8,9},{9,8},{10,11... | collective-permute-start | bytes 1572872 | tf_op jit(solution)/shard_map/ppermute | solution.py:262
  16.2 30.0 %collective-permute-start.1 = (bf16[256,1024]{1,0:T(8,128)(2,1)}, bf16[256,1024]{1,0:T(8,128)(2,1)S(1)}, u32[]{:S(2)}, u32[]{:S(2)}) collective-permute-start(bf16[256,1024]{1,0:T(8,128)(2,1)} %bitcast.22), channel_id=1, source_target_pairs={{0,1},{1,0},{2,3},{3,2},{4,5},{5,4},{6,7},{7,6},{8,9},{9,8},{10,11... | collective-permute-start | bytes 1572872 | tf_op jit(solution)/shard_map/ppermute | solution.py:263
  20.3 0.7 copy-start.6
  22.3 10.7 %copy-start.8 = (f32[32,8]{0,1:T(8,128)S(1)}, f32[32,8]{0,1:T(8,128)}, u32[]{:S(2)}) copy-start(f32[32,8]{0,1:T(8,128)} %param.14) | copy-start | bytes 3076
  22.3 10.7 %copy-start.10 = (f32[256]{0:T(256)S(1)}, f32[256]{0:T(256)}, u32[]{:S(2)}) copy-start(f32[256]{0:T(256)} %param.21) | copy-start | bytes 3076
  22.3 23.8 %all-to-all-start = ((bf16[64,8,256]{2,1,0:T(8,128)(2,1)}), bf16[64,8,256]{2,1,0:T(8,128)(2,1)S(1)}, u32[]{:S(2)}, u32[]{:S(2)}) async-start(bf16[64,8,256]{2,1,0:T(8,128)(2,1)} %bitcast.3), calls=%async_computation | async-start | bytes 524288 | tf_op jit(solution)/shard_map/all_to_all | solution.py:259
  32.9 0.7 copy-start.7
  32.9 0.7 copy-start.9
  33.6 1.0 copy-start.1
  34.7 11.5 %copy-start.2 = (bf16[1,256,1024]{2,1,0:T(8,128)(2,1)S(1)}, bf16[1,256,1024]{2,1,0:T(8,128)(2,1)}, u32[]{:S(2)}) copy-start(bf16[1,256,1024]{2,1,0:T(8,128)(2,1)} %param.15) | copy-start | bytes 1572868
  34.7 11.5 %copy-start.3 = (bf16[1,256,1024]{2,1,0:T(8,128)(2,1)S(1)}, bf16[1,256,1024]{2,1,0:T(8,128)(2,1)}, u32[]{:S(2)}) copy-start(bf16[1,256,1024]{2,1,0:T(8,128)(2,1)} %param.16) | copy-start | bytes 1572868
  35.2 3.4 %collective-permute-start.2 = (bf16[9,16,256]{2,1,0:T(8,128)(2,1)S(1)}, bf16[9,16,256]{2,1,0:T(8,128)(2,1)S(1)}, u32[]{:S(2)}, u32[]{:S(2)}) collective-permute-start(bf16[9,16,256]{2,1,0:T(8,128)(2,1)S(1)} %get-tuple-element.14), channel_id=1, source_target_pairs={{0,1},{1,0},{2,3},{3,2},{4,5},{5,4},{6,7},{7,6},{8,9},{9,8},{10,11... | collective-permute-start | bytes 221192 | tf_op jit(solution)/shard_map/ppermute | solution.py:282
  75.2 21.5 %copy-start.5 = (bf16[1024,256]{1,0:T(8,128)(2,1)S(1)}, bf16[1024,256]{1,0:T(8,128)(2,1)}, u32[]{:S(2)}) copy-start(bf16[1024,256]{1,0:T(8,128)(2,1)} %shared_down_ref.1) | copy-start | bytes 1572868
  75.4 21.3 %copy-start.4 = (bf16[1,1024,256]{2,1,0:T(8,128)(2,1)S(1)}, bf16[1,1024,256]{2,1,0:T(8,128)(2,1)}, u32[]{:S(2)}) copy-start(bf16[1,1024,256]{2,1,0:T(8,128)(2,1)} %param.17) | copy-start | bytes 1572868

commit v3 on v2

--- a/solution.py
+++ b/solution.py
@@ -84,34 +84,67 @@
         out_ref[n] = part.astype(bf16)
 
 
-def shared_up_kernel(
+def swap_kernel(
     core_ref,
     both_ref,
     gain_ref,
     gate_ref,
     up_ref,
+    shared_gate_ref,
+    shared_up_ref,
     routes_ref,
     weights_ref,
     out_gain_ref,
+    swap_ref,
     keep_ref,
-    send_ref,
     combine_ref,
     later_gain_ref,
+    own_gain,
+    shared_gate,
+    shared_up,
+    routes,
+    weights,
+    sems,
 ):
-    later_gain_ref[...] = out_gain_ref[...]
-    combine_weights(routes_ref, weights_ref, combine_ref)
-    first = core_ref[0] == 0
-    rows = (both_ref[core_ref[0]].astype(f32) * gain_ref[...]).astype(bf16)
+    depth = gate_ref.shape[0]
+    pairs = (
+        (routes_ref, routes),
+        (weights_ref, weights),
+        (gain_ref, own_gain),
+        (shared_gate_ref, shared_gate),
+        (shared_up_ref, shared_up),
+        (out_gain_ref, later_gain_ref),
+        (gate_ref, swap_ref.at[:depth]),
+        (up_ref, swap_ref.at[depth : 2 * depth]),
+    )
+    copies = [pltpu.make_async_copy(a, b, sems.at[n]) for n, (a, b) in enumerate(pairs)]
+    for copy in copies:
+        copy.start()
+    core = core_ref[0]
+    first = core == 0
+    for copy in copies[:3]:
+        copy.wait()
+    combine_weights(routes, weights, combine_ref)
+    gain = own_gain[...]
+    rows = (both_ref[core].astype(f32) * gain).astype(bf16)
     half = rows.shape[0] // 2
+    parts = three_parts(gain)
+    line = iota((8, gain.shape[1]), 0)
+    gain = jnp.where(line == 0, parts[0], jnp.where(line == 1, parts[1], parts[2]))
+    gain = jnp.where(line < 3, gain, 0.0).astype(bf16)
+    swap_ref[2 * depth + 2 * half :] = jnp.concatenate([gain] * 4, axis=1)
+    for copy in copies[3:5]:
+        copy.wait()
     for n in range(keep_ref.shape[0]):
         cut = slice(n * 128, (n + 1) * 128)
-        part = dot(rows, jnp.concatenate([gate_ref[:, cut], up_ref[:, cut]], axis=1))
+        part = dot(rows, jnp.concatenate([shared_gate[:, cut], shared_up[:, cut]], axis=1))
         keep_ref[n] = jnp.where(first, part[:half], part[half:])
-        send_ref[n] = jnp.where(first, part[half:], part[:half]).astype(bf16)
-    parts = three_parts(gain_ref[...])
-    line = iota(send_ref.shape[1:], 0)
-    gain = jnp.where(line == 0, parts[0], jnp.where(line == 1, parts[1], parts[2]))
-    send_ref[keep_ref.shape[0]] = jnp.where(line < 3, gain, 0.0).astype(bf16)
+        at, lane = 2 * depth + n // 4 * half, n % 4 * 256
+        swap_ref[at : at + half, lane : lane + 256] = jnp.where(
+            first, part[half:], part[:half]
+        ).astype(bf16)
+    for copy in copies[5:]:
+        copy.wait()
 
 
 def hidden_parts_kernel(
@@ -119,12 +152,9 @@
     rows_ref,
     both_ref,
     gain_ref,
-    gate_ref,
-    up_ref,
-    gate_other_ref,
-    up_other_ref,
+    near_ref,
+    far_ref,
     kept_ref,
-    sent_ref,
     out_ref,
 ):
     first = core_ref[0] == 0
@@ -136,8 +166,8 @@
     own = dot(jnp.where(at == place, 1.0, 0.0).astype(bf16), arrived)
     other = dot(jnp.where(at == place + 4, 1.0, 0.0).astype(bf16), arrived)
     squares = jnp.sum(own * own + other * other, axis=1, keepdims=True)
-    near, far = both_ref[0].astype(f32), both_ref[1].astype(f32)
-    token_squares = jnp.sum(near * near + far * far, axis=1, keepdims=True)
+    low, high = both_ref[0].astype(f32), both_ref[1].astype(f32)
+    token_squares = jnp.sum(low * low + high * high, axis=1, keepdims=True)
     half = token_squares.shape[0] // 2
     token_squares = jnp.where(first, token_squares[:half], token_squares[half:])
     squares = jnp.concatenate([squares, token_squares], axis=0) * (1.0 / D)
@@ -146,16 +176,19 @@
     extra = jnp.where(line == 0, parts[0], jnp.where(line == 1, parts[1], parts[2]))
     extra = jnp.where(line < 3, extra, 0.0).astype(bf16)
     own = (own * gain_ref[...]).astype(bf16)
-    swapped = sent_ref[out_ref.shape[0]].astype(f32)
+    depth = gain_ref.shape[1]
+    shared_at = 2 * depth
+    swapped = far_ref[shared_at + 2 * half :, :depth].astype(f32)
     gain_other = swapped[0:1] + swapped[1:2] + swapped[2:3]
     other = (other * gain_other).astype(bf16)
     for n in range(out_ref.shape[0]):
         cut = slice(n * 128, (n + 1) * 128)
-        part = dot(own, jnp.concatenate([gate_ref[:, cut], up_ref[:, cut]], axis=1)) + dot(
-            other, jnp.concatenate([gate_other_ref[:, cut], up_other_ref[:, cut]], axis=1)
-        )
-        out_ref[n, :slots] = part.astype(bf16)
-        out_ref[n, slots : slots + half] = (kept_ref[n] + sent_ref[n].astype(f32)).astype(bf16)
+        near = jnp.concatenate([near_ref[:depth, cut], near_ref[depth:shared_at, cut]], axis=1)
+        far = jnp.concatenate([far_ref[:depth, cut], far_ref[depth:shared_at, cut]], axis=1)
+        out_ref[n, :slots] = (dot(own, near) + dot(other, far)).astype(bf16)
+        at, lane = shared_at + n // 4 * half, n % 4 * 256
+        given = far_ref[at : at + half, lane : lane + 256].astype(f32)
+        out_ref[n, slots : slots + half] = (kept_ref[n] + given).astype(bf16)
         out_ref[n, slots + half :] = extra
 
 
@@ -209,18 +242,25 @@
     out_ref[...] = (mixed_ref[...] * scale).astype(bf16)
 
 
-def call(body, out, *operands, flops=0):
-    def spec(array):
+def call(body, out, *operands, flops=0, far=(), scratch=()):
+    def spec(n, array):
+        if n in far:
+            return pl.BlockSpec(memory_space=pltpu.HBM)
         return pl.BlockSpec(memory_space=pltpu.SMEM if array.shape == (1,) else pltpu.VMEM)
 
+    operands = [
+        pltpu.with_memory_space_constraint(a, pltpu.HBM) if n in far else a
+        for n, a in enumerate(operands)
+    ]
     outs = out if isinstance(out, tuple) else (out,)
     specs = tuple(pl.BlockSpec(memory_space=pltpu.VMEM) for _ in outs)
     moved = sum(a.size * a.dtype.itemsize for a in (*operands, *outs))
     return pl.pallas_call(
         body,
         out_shape=out,
-        in_specs=[spec(a) for a in operands],
+        in_specs=[spec(n, a) for n, a in enumerate(operands)],
         out_specs=specs if isinstance(out, tuple) else specs[0],
+        scratch_shapes=scratch,
         compiler_params=pltpu.CompilerParams(vmem_limit_bytes=24 * MIB),
         cost_estimate=pl.CostEstimate(flops=flops, bytes_accessed=moved, transcendentals=0),
     )(*operands)
@@ -259,27 +299,36 @@
     arrived = lax.all_to_all(
         outgoing.reshape(sources, 8, features), "ep", 0, 0, tiled=True
     )
-    gate_other = lax.ppermute(gate, "core", swap)
-    up_other = lax.ppermute(up, "core", swap)
-    kept, given, weights, later_gain = call(
-        shared_up_kernel,
+    near, kept, weights, later_gain = call(
+        swap_kernel,
         (
+            shape((2 * features + 2 * half + 8, 1024), bf16),
             shape((lines, half, 256), f32),
-            shape((lines + 1, half, 256), bf16),
             shape((3, rows, sent), bf16),
             shape((1, features), f32),
         ),
         core,
         both,
         gain,
+        gate,
+        up,
         shared_gate,
         shared_up,
         routes,
         route_weights,
         out_gain.reshape(1, features),
         flops=2 * rows * features * 2048,
-    )
-    taken = lax.ppermute(given, "core", swap)
+        far=range(2, 10),
+        scratch=[
+            pltpu.VMEM((1, features), f32),
+            pltpu.VMEM((features, 1024), bf16),
+            pltpu.VMEM((features, 1024), bf16),
+            pltpu.VMEM(routes.shape, i32),
+            pltpu.VMEM(route_weights.shape, f32),
+            pltpu.SemaphoreType.DMA((8,)),
+        ],
+    )
+    far = lax.ppermute(near, "core", swap)
 
     parts = call(
         hidden_parts_kernel,
@@ -288,12 +337,9 @@
         arrived.reshape(sent, features),
         both,
         gain,
-        gate,
-        up,
-        gate_other,
-        up_other,
+        near,
+        far,
         kept,
-        taken,
         flops=4 * slots * features * 2048,
     )
     parts = lax.all_to_all(parts, "x", 0, 0, tiled=True)

time: 131 us -> 128 us (0.977)
  blocking collectives: 83.3 us -> 121 us
  starting transfers between devices: 31.3 us -> 2.26 us
  waiting for transfers between devices: 8.37 us -> 0.01 us
  local copies, waits for them, and re-layouts: 2.41 us -> 0.01 us
    all_to_all x0 -> x1, blocking collectives: none -> 23.7 us  [per_device(): lax.all_to_all(outgoing.reshape(sources, 8, features), 'ep', 0, 0, tiled=...]
    ppermute x3 -> x1, starting transfers between devices: 20.6 us -> 2.26 us  [per_device(): far = lax.ppermute(near, 'core', swap)]
    all_gather x1, blocking collectives: 2.19 us -> 15.9 us  [per_device(): both = lax.all_gather(tokens, 'core', axis=0)]
    all_to_all x1 -> x0, starting transfers between devices: 10.6 us -> none  [per_device(): lax.all_to_all(outgoing.reshape(sources, 8, features), 'ep', 0, 0, tiled=...]
    all_to_all x1 -> x0, waiting for transfers between devices: 7.47 us -> none  [per_device(): lax.all_to_all(outgoing.reshape(sources, 8, features), 'ep', 0, 0, tiled=...]
    unnamed x22 -> x8, local copies, waits for them, and re-layouts: 2.41 us -> 0.01 us
  transfers between devices with their start and end apart: 4 -> 1, of which waited for: 2 -> 0; matrix products, arithmetic and copies ran while one was open for 0% -> 0% of each run, Pallas kernels for 1% -> 0%
where the time goes in v3:
time: 128 us
  blocking collectives  121 us (95%)
  Pallas kernels  5.09 us (4%)
  starting transfers between devices  2.26 us (2%)
    all_to_all x1, blocking collectives, per_device(): parts = lax.all_to_all(parts, 'x', 0, 0, tiled=True)  28.4 us
    all_to_all x1, blocking collectives, per_device(): lax.all_to_all(outgoing.reshape(sources, 8, features), 'ep', 0, 0, tiled=...  23.7 us
    all_gather x1, blocking collectives, per_device(): hidden = lax.all_gather(hidden, ('x', 'core'), axis=0)  21.1 us
    all_to_all x1, blocking collectives, per_device(): lax.all_to_all(leaving.reshape(sources, 8, features), 'ep', 0, 0, tiled=T...  18.3 us
    all_gather x1, blocking collectives, per_device(): both = lax.all_gather(tokens, 'core', axis=0)  15.9 us
    all_to_all x1, blocking collectives, per_device(): squares = lax.all_to_all(squares, ('x', 'core'), 0, 0, tiled=True)  13.1 us
    pallas_call x7, Pallas kernels, call(): pl.pallas_call(body, out_shape=out, in_specs=[spec(n, a) for n, a in enum...  5.09 us
  transfers between devices with their start and end apart: 1, of which 0 were waited for; matrix products, arithmetic and copies ran while one was open for 0% of the time, Pallas kernels for 0%

profile of v3, /device:TPU:1, one launch (start us, length us, event | category | flops | bytes accessed | tf_op | source)
XLA Modules:
  0.0 128.0 jit_solution(8575623303968398814)
XLA Ops:
  0.0 0.0 copy-start.2
  0.0 15.9 %all-gather = bf16[64,256]{1,0:T(8,128)(2,1)S(1)} all-gather(bf16[32,256]{1,0:T(8,128)(2,1)} %param.11), channel_id=2, replica_groups=mesh['ep'=64,'x'=8,'core'=2] {'core'}, dimensions={0}, use_global_device_ids=true | all-gather | bytes 49152 | tf_op jit(solution)/shard_map/all_gather | solution.py:297
  15.9 0.0 copy-start.3
  15.9 1.7 %shard_map.110 = (bf16[552,1024]{1,0:T(8,128)(2,1)S(1)}, f32[8,16,256]{2,1,0:T(8,128)S(1)}, bf16[3,32,512]{2,1,0:T(8,128)(2,1)S(1)}, f32[1,256]{1,0:T(1,128)S(1)}) custom-call(s32[1]{0:T(128)} %bitcast.core_ref, bf16[2,32,256]{2,1,0:T(8,128)(2,1)S(1)} %bitcast.18, f32[1,256]{1,0:T(1,128)} %bitcast.25, bf16[256,1024]{1,0:T(8,128)(2,1)} %bitcast.27, ...), custom_call_target="tpu_custom_call" | custom-call | flops 33554432 | bytes 3494916 | tf_op jit(solution)/shard_map/pallas_call | solution.py:258
  17.6 2.3 %collective-permute-start = (bf16[552,1024]{1,0:T(8,128)(2,1)S(1)}, bf16[552,1024]{1,0:T(8,128)(2,1)S(1)}, u32[]{:S(2)}, u32[]{:S(2)}) collective-permute-start(bf16[552,1024]{1,0:T(8,128)(2,1)S(1)} %get-tuple-element.13.near_ref), channel_id=1, source_target_pairs={{0,1},{1,0},{2,3},{3,2},{4,5},{5,4},{6,7},{7,6},{8,9},{9,8},{10,11... | collective-permute-start | bytes 3391496 | tf_op jit(solution)/shard_map/ppermute | solution.py:331
  19.9 0.0 copy-done.2
  19.9 0.6 shard_map.109
  20.5 23.7 %all_to_all.20 = bf16[64,8,256]{2,1,0:T(8,128)(2,1)S(1)} all-to-all(bf16[64,8,256]{2,1,0:T(8,128)(2,1)S(1)} %bitcast.17), channel_id=1, replica_groups=mesh['ep'=64,'x'=8,'core'=2] {'ep'}, dimensions={0} | all-to-all | bytes 524288 | tf_op jit(solution)/shard_map/all_to_all | solution.py:299
  44.2 0.0 collective-permute-done.far_ref
  44.2 0.0 copy-done.3
  44.2 0.9 shard_map.111
  45.1 28.4 %all_to_all.21.parts_ref = bf16[8,216,256]{2,1,0:T(8,128)(2,1)S(1)} all-to-all(bf16[8,216,256]{2,1,0:T(8,128)(2,1)S(1)} %shard_map.111), channel_id=1, replica_groups=mesh['ep'=64,'x'=8,'core'=2] {'x'}, dimensions={0} | all-to-all | bytes 1769472 | tf_op jit(solution)/shard_map/all_to_all | solution.py:345
  73.5 0.0 copy-start
  73.5 0.0 copy-start.1
  73.5 0.2 shard_map.112
  73.7 21.1 %all-gather.1 = bf16[3328,128]{1,0:T(8,128)(2,1)S(1)} all-gather(bf16[208,128]{1,0:T(8,128)(2,1)S(1)} %shard_map.112), channel_id=3, replica_groups=mesh['ep'=64,'x'=8,'core'=2] {'x','core'}, dimensions={0}, use_global_device_ids=true | all-gather | bytes 905216 | tf_op jit(solution)/shard_map/all_gather | solution.py:347
  94.7 0.0 copy-done
  94.7 0.0 copy-done.1
  94.8 0.7 shard_map.113
  95.5 18.3 %all_to_all.22 = bf16[64,8,256]{2,1,0:T(8,128)(2,1)S(1)} all-to-all(bf16[64,8,256]{2,1,0:T(8,128)(2,1)S(1)} %bitcast.22), channel_id=1, replica_groups=mesh['ep'=64,'x'=8,'core'=2] {'ep'}, dimensions={0} | all-to-all | bytes 524288 | tf_op jit(solution)/shard_map/all_to_all | solution.py:356
  113.8 0.3 shard_map.114
  114.1 13.1 %all_to_all.23.squares_ref = f32[16,1,128]{2,1,0:T(1,128)S(1)} all-to-all(f32[16,1,128]{2,1,0:T(1,128)S(1)} %get-tuple-element.19), channel_id=1, replica_groups=mesh['ep'=64,'x'=8,'core'=2] {'x','core'}, dimensions={0} | all-to-all | bytes 16384 | tf_op jit(solution)/shard_map/all_to_all | solution.py:365
  127.3 0.7 shard_map.115
Async XLA Ops:
  0.0 19.9 %copy-start.2 = (s32[32,8]{0,1:T(8,128)S(1)}, s32[32,8]{0,1:T(8,128)}, u32[]{:S(2)}) copy-start(s32[32,8]{0,1:T(8,128)} %param.13) | copy-start | bytes 3076
  15.9 28.3 %copy-start.3 = (f32[256]{0:T(256)S(1)}, f32[256]{0:T(256)}, u32[]{:S(2)}) copy-start(f32[256]{0:T(256)} %param.12) | copy-start | bytes 3076
  17.6 26.6 %collective-permute-start = (bf16[552,1024]{1,0:T(8,128)(2,1)S(1)}, bf16[552,1024]{1,0:T(8,128)(2,1)S(1)}, u32[]{:S(2)}, u32[]{:S(2)}) collective-permute-start(bf16[552,1024]{1,0:T(8,128)(2,1)S(1)} %get-tuple-element.13.near_ref), channel_id=1, source_target_pairs={{0,1},{1,0},{2,3},{3,2},{4,5},{5,4},{6,7},{7,6},{8,9},{9,8},{10,11... | collective-permute-start | bytes 3391496 | tf_op jit(solution)/shard_map/ppermute | solution.py:331
  73.5 21.3 %copy-start = (bf16[1,1024,256]{2,1,0:T(8,128)(2,1)S(1)}, bf16[1,1024,256]{2,1,0:T(8,128)(2,1)}, u32[]{:S(2)}) copy-start(bf16[1,1024,256]{2,1,0:T(8,128)(2,1)} %param.17) | copy-start | bytes 1572868
  73.5 21.3 %copy-start.1 = (bf16[1024,256]{1,0:T(8,128)(2,1)S(1)}, bf16[1024,256]{1,0:T(8,128)(2,1)}, u32[]{:S(2)}) copy-start(bf16[1024,256]{1,0:T(8,128)(2,1)} %shared_down_ref.1) | copy-start | bytes 1572868

commit v4 on v3

--- a/solution.py
+++ b/solution.py
@@ -41,31 +41,29 @@
 
 def named_slots(routes, lanes):
     rows, picks = routes.shape
-    expert = iota((rows, lanes), 1) >> 3
+    lane = iota((rows, lanes), 1)
+    expert = (lane * 43691) >> 19
     named = routes[:, 0:1] == expert
     for k in range(1, picks):
         named = named | (routes[:, k : k + 1] == expert)
     earlier = (iota((rows, rows), 1) < iota((rows, rows), 0)).astype(f32).astype(bf16)
     rank = dot(earlier, jnp.where(named, 1.0, 0.0).astype(bf16))
-    return named, rank.astype(i32)
+    return named, rank.astype(i32), expert, lane - 12 * expert
+
+
+def quarters(core, both_ref):
+    own, other = both_ref[core], both_ref[1 - core]
+    return own[:, :128], own[:, 128:], other[:, :128], other[:, 128:]
 
 
 def pack_kernel(core_ref, routes_ref, both_ref, out_ref):
     core = core_ref[0]
-    lanes = out_ref.shape[0]
-    named, rank = named_slots(routes_ref[...].T, lanes)
-    lane = iota(named.shape, 1)
-    slot = lane & 3
-    chosen = named & (rank == 3 * core + slot) & (slot < 3)
-    other = (lane & 4) > 0
+    named, rank, _, line = named_slots(routes_ref[...].T, out_ref.shape[0])
+    chosen = jnp.where(named & (rank == 3 * core + (line >> 2)), 1.0, 0.0)
     picks = jnp.concatenate(
-        [
-            jnp.where(chosen & ~other, 1.0, 0.0).astype(bf16),
-            jnp.where(chosen & other, 1.0, 0.0).astype(bf16),
-        ],
-        axis=0,
-    )
-    rows = jnp.concatenate([both_ref[core], both_ref[1 - core]], axis=0)
+        [jnp.where((line & 3) == q, chosen, 0.0).astype(bf16) for q in range(4)], axis=0
+    )
+    rows = jnp.concatenate(quarters(core, both_ref), axis=0)
     out_ref[...] = lax.dot_general(
         picks, rows, (((0,), (0,)), ((), ())), preferred_element_type=f32
     ).astype(bf16)
@@ -73,15 +71,18 @@
 
 def combine_weights(routes_ref, weights_ref, out_ref):
     routes, given = routes_ref[...].T, weights_ref[...].T
-    lanes = out_ref.shape[2]
-    named, rank = named_slots(routes, lanes)
-    lane = iota(named.shape, 1)
+    named, rank, expert, line = named_slots(routes, out_ref.shape[1])
     weight = jnp.zeros(named.shape, f32)
     for k in range(routes.shape[1]):
-        weight = jnp.where(routes[:, k : k + 1] == lane >> 3, given[:, k : k + 1], weight)
-    weight = jnp.where(named & (rank == (lane & 7)), weight, 0.0)
-    for n, part in enumerate(three_parts(weight)):
-        out_ref[n] = part.astype(bf16)
+        weight = jnp.where(routes[:, k : k + 1] == expert, given[:, k : k + 1], weight)
+    slot = 3 * ((line >> 1) & 1) + (line >> 2)
+    weight = jnp.where(named & (rank == slot), weight, 0.0)
+    rows = weight.shape[0]
+    at = 0
+    for part in three_parts(weight):
+        for side in range(2):
+            out_ref[at : at + rows] = jnp.where((line & 1) == side, part, 0.0).astype(bf16)
+            at += rows
 
 
 def swap_kernel(
@@ -156,15 +157,15 @@
     far_ref,
     kept_ref,
     out_ref,
+    wide,
 ):
     first = core_ref[0] == 0
-    arrived = rows_ref[...]
-    slots = 3 * arrived.shape[0] // 8
-    sources = arrived.shape[0] // 8
-    to, at = iota((slots, arrived.shape[0]), 0), iota((slots, arrived.shape[0]), 1)
-    place = (to % sources) * 8 + to // sources
-    own = dot(jnp.where(at == place, 1.0, 0.0).astype(bf16), arrived)
-    other = dot(jnp.where(at == place + 4, 1.0, 0.0).astype(bf16), arrived)
+    slots = rows_ref.shape[0] // 4
+    wide[...] = rows_ref[...].astype(f32)
+    own, other = (
+        jnp.concatenate([wide[pl.ds(q, slots, stride=4), :] for q in pair], axis=1)
+        for pair in ((0, 1), (2, 3))
+    )
     squares = jnp.sum(own * own + other * other, axis=1, keepdims=True)
     low, high = both_ref[0].astype(f32), both_ref[1].astype(f32)
     token_squares = jnp.sum(low * low + high * high, axis=1, keepdims=True)
@@ -208,17 +209,16 @@
     return jnp.concatenate([ref[n, lo:hi] for n in range(core, ref.shape[0], 2)], axis=1)
 
 
-def down_kernel(hidden_ref, down_ref, shared_down_ref, out_ref, shared_ref):
-    sent = out_ref.shape[0]
-    slots = 3 * sent // 8
+def down_kernel(hidden_ref, down_ref, shared_down_ref, out_ref, shared_ref, wide):
+    slots = out_ref.shape[0] // 4
     down = down_ref[...]
-    rows = jnp.concatenate(
-        [dot(lanes_of(hidden_ref, core, 0, slots), down).astype(bf16) for core in range(2)], axis=0
-    )
-    to, at = iota((sent, 2 * slots), 0), iota((sent, 2 * slots), 1)
-    place = (to & 7) * (sent // 8) + (to >> 3)
-    out_ref[...] = dot(jnp.where(at == place, 1.0, 0.0).astype(bf16), rows).astype(bf16)
-
+    for core in range(2):
+        rows = dot(lanes_of(hidden_ref, core, 0, slots), down)
+        for side in range(2):
+            wide[pl.ds(2 * core + side, slots, stride=4), :] = rows[
+                :, side * 128 : (side + 1) * 128
+            ]
+    out_ref[...] = wide[...].astype(bf16)
     end = hidden_ref.shape[1]
     hidden = jnp.concatenate(
         [lanes_of(hidden_ref, core, slots, end) for core in range(2)], axis=0
@@ -227,10 +227,13 @@
 
 
 def combine_kernel(rows_ref, weights_ref, shared_ref, gain_ref, mixed_ref, squares_ref):
-    rows = rows_ref[...]
-    mixed = shared_ref[...]
-    for n in range(3):
-        mixed = mixed + dot(weights_ref[n], rows)
+    parts = dot(weights_ref[...], rows_ref[...])
+    count = shared_ref.shape[0]
+    low, high = (
+        sum(parts[at * count : (at + 1) * count] for at in (side, side + 2, side + 4))
+        for side in range(2)
+    )
+    mixed = shared_ref[...] + jnp.concatenate([low, high], axis=1)
     mixed_ref[...] = mixed * gain_ref[...]
     squares = to_row(jnp.sum(mixed * mixed, axis=1, keepdims=True), 128)
     squares_ref[...] = jnp.broadcast_to(squares[None], squares_ref.shape)
@@ -270,6 +273,11 @@
     return jax.ShapeDtypeStruct(dims, dtype)
 
 
+def exchanged(rows, sources):
+    blocks = rows.reshape(sources, -1, 4, 128)
+    return lax.all_to_all(blocks, "ep", 0, 0, tiled=True).reshape(rows.shape)
+
+
 def per_device(
     tokens,
     norm_gain,
@@ -285,7 +293,7 @@
 ):
     rows, features = tokens.shape
     sources, lines, cores = (lax.axis_size(a) for a in ("ep", "x", "core"))
-    sent = sources * 8
+    sent = sources * 12
     slots = sources * 3
     half = rows // 2
     core = lax.axis_index("core").astype(i32).reshape(1)
@@ -295,16 +303,14 @@
 
     routes, route_weights = routes.T, route_weights.T
     both = lax.all_gather(tokens, "core", axis=0)
-    outgoing = call(pack_kernel, shape((sent, features), bf16), core, routes, both)
-    arrived = lax.all_to_all(
-        outgoing.reshape(sources, 8, features), "ep", 0, 0, tiled=True
-    )
+    outgoing = call(pack_kernel, shape((sent, 128), bf16), core, routes, both)
+    arrived = exchanged(outgoing, sources)
     near, kept, weights, later_gain = call(
         swap_kernel,
         (
             shape((2 * features + 2 * half + 8, 1024), bf16),
             shape((lines, half, 256), f32),
-            shape((3, rows, sent), bf16),
+            shape((6 * rows, sent), bf16),
             shape((1, features), f32),
         ),
         core,
@@ -334,30 +340,32 @@
         hidden_parts_kernel,
         shape((lines, slots + half + 8, 256), bf16),
         core,
-        arrived.reshape(sent, features),
+        arrived,
         both,
         gain,
         near,
         far,
         kept,
         flops=4 * slots * features * 2048,
+        scratch=[pltpu.VMEM((sent, 128), f32)],
     )
     parts = lax.all_to_all(parts, "x", 0, 0, tiled=True)
     hidden = call(hidden_kernel, shape((slots + half, 128), bf16), parts)
     hidden = lax.all_gather(hidden, ("x", "core"), axis=0)
     leaving, shared = call(
         down_kernel,
-        (shape((sent, features), bf16), shape((rows, features), f32)),
+        (shape((sent, 128), bf16), shape((rows, features), f32)),
         hidden,
         down,
         shared_down,
+        scratch=[pltpu.VMEM((sent, 128), f32)],
         flops=4 * slots * 1024 * features,
     )
-    returned = lax.all_to_all(leaving.reshape(sources, 8, features), "ep", 0, 0, tiled=True)
+    returned = exchanged(leaving, sources)
     mixed, squares = call(
         combine_kernel,
         (shape((rows, features), f32), shape((lines * cores, 1, 128), f32)),
-        returned.reshape(sent, features),
+        returned,
         weights,
         shared,
         later_gain,

time: 128 us -> 125 us (0.977)
  blocking collectives: 121 us -> 118 us
    all_to_all x2, blocking collectives: 42.1 us -> 39.7 us  [exchanged(): return lax.all_to_all(blocks, 'ep', 0, 0, tiled=True).reshape(rows.shape)]
where the time goes in v4:
time: 125 us
  blocking collectives  118 us (94%)
  Pallas kernels  4.53 us (4%)
  starting transfers between devices  2.26 us (2%)
    all_to_all x2, blocking collectives, exchanged(): return lax.all_to_all(blocks, 'ep', 0, 0, tiled=True).reshape(rows.shape)  39.7 us
    all_to_all x1, blocking collectives, per_device(): parts = lax.all_to_all(parts, 'x', 0, 0, tiled=True)  28.5 us
    all_gather x1, blocking collectives, per_device(): hidden = lax.all_gather(hidden, ('x', 'core'), axis=0)  21 us
    all_gather x1, blocking collectives, per_device(): both = lax.all_gather(tokens, 'core', axis=0)  15.9 us
    all_to_all x1, blocking collectives, per_device(): squares = lax.all_to_all(squares, ('x', 'core'), 0, 0, tiled=True)  13 us
    pallas_call x7, Pallas kernels, call(): pl.pallas_call(body, out_shape=out, in_specs=[spec(n, a) for n, a in enum...  4.53 us
  transfers between devices with their start and end apart: 1, of which 0 were waited for; matrix products, arithmetic and copies ran while one was open for 0% of the time, Pallas kernels for 0%

profile of v4, /device:TPU:1, one launch (start us, length us, event | category | flops | bytes accessed | tf_op | source)
XLA Modules:
  0.0 125.0 jit_solution(8746321454358427872)
XLA Ops:
  0.0 0.0 copy-start.2
  0.0 15.9 %all-gather = bf16[64,256]{1,0:T(8,128)(2,1)S(1)} all-gather(bf16[32,256]{1,0:T(8,128)(2,1)} %param.11), channel_id=2, replica_groups=mesh['ep'=64,'x'=8,'core'=2] {'core'}, dimensions={0}, use_global_device_ids=true | all-gather | bytes 49152 | tf_op jit(solution)/shard_map/all_gather | solution.py:305
  15.9 0.0 copy-start.3
  15.9 1.7 %shard_map.110 = (bf16[552,1024]{1,0:T(8,128)(2,1)S(1)}, f32[8,16,256]{2,1,0:T(8,128)S(1)}, bf16[192,768]{1,0:T(8,128)(2,1)S(1)}, f32[1,256]{1,0:T(1,128)S(1)}) custom-call(s32[1]{0:T(128)} %bitcast.core_ref, bf16[2,32,256]{2,1,0:T(8,128)(2,1)S(1)} %bitcast.18, f32[1,256]{1,0:T(1,128)} %bitcast.25, bf16[256,1024]{1,0:T(8,128)(2,1)} %bitcast.27, ...), custom_call_target="tpu_custom_call" | custom-call | flops 33554432 | bytes 3691524 | tf_op jit(solution)/shard_map/pallas_call | solution.py:261
  17.6 2.3 %collective-permute-start = (bf16[552,1024]{1,0:T(8,128)(2,1)S(1)}, bf16[552,1024]{1,0:T(8,128)(2,1)S(1)}, u32[]{:S(2)}, u32[]{:S(2)}) collective-permute-start(bf16[552,1024]{1,0:T(8,128)(2,1)S(1)} %get-tuple-element.13.near_ref), channel_id=1, source_target_pairs={{0,1},{1,0},{2,3},{3,2},{4,5},{5,4},{6,7},{7,6},{8,9},{9,8},{10,11... | collective-permute-start | bytes 3391496 | tf_op jit(solution)/shard_map/ppermute | solution.py:337
  19.9 0.0 copy-done.2
  19.9 0.6 shard_map.109
  20.5 22.7 %all_to_all.20 = bf16[64,3,4,128]{3,2,1,0:T(4,128)(2,1)S(1)} all-to-all(bf16[64,3,4,128]{3,2,1,0:T(4,128)(2,1)S(1)} %bitcast.16), channel_id=1, replica_groups=mesh['ep'=64,'x'=8,'core'=2] {'ep'}, dimensions={0} | all-to-all | bytes 393216 | tf_op jit(solution)/shard_map/all_to_all | solution.py:278
  43.2 0.0 collective-permute-done.far_ref
  43.2 0.0 copy-done.3
  43.2 0.6 shard_map.111
  43.8 28.5 %all_to_all.21.parts_ref = bf16[8,216,256]{2,1,0:T(8,128)(2,1)S(1)} all-to-all(bf16[8,216,256]{2,1,0:T(8,128)(2,1)S(1)} %shard_map.111), channel_id=1, replica_groups=mesh['ep'=64,'x'=8,'core'=2] {'x'}, dimensions={0} | all-to-all | bytes 1769472 | tf_op jit(solution)/shard_map/all_to_all | solution.py:352
  72.2 0.0 copy-start
  72.2 0.0 copy-start.1
  72.3 0.2 shard_map.112
  72.4 21.0 %all-gather.1 = bf16[3328,128]{1,0:T(8,128)(2,1)S(1)} all-gather(bf16[208,128]{1,0:T(8,128)(2,1)S(1)} %shard_map.112), channel_id=3, replica_groups=mesh['ep'=64,'x'=8,'core'=2] {'x','core'}, dimensions={0}, use_global_device_ids=true | all-gather | bytes 905216 | tf_op jit(solution)/shard_map/all_gather | solution.py:354
  93.4 0.0 copy-done
  93.4 0.0 copy-done.1
  93.4 0.5 shard_map.113
  93.9 17.0 %all_to_all.22 = bf16[64,3,4,128]{3,2,1,0:T(4,128)(2,1)S(1)} all-to-all(bf16[64,3,4,128]{3,2,1,0:T(4,128)(2,1)S(1)} %bitcast.22), channel_id=1, replica_groups=mesh['ep'=64,'x'=8,'core'=2] {'ep'}, dimensions={0} | all-to-all | bytes 393216 | tf_op jit(solution)/shard_map/all_to_all | solution.py:278
  110.9 0.3 shard_map.114
  111.2 13.0 %all_to_all.23.squares_ref = f32[16,1,128]{2,1,0:T(1,128)S(1)} all-to-all(f32[16,1,128]{2,1,0:T(1,128)S(1)} %get-tuple-element.19), channel_id=1, replica_groups=mesh['ep'=64,'x'=8,'core'=2] {'x','core'}, dimensions={0} | all-to-all | bytes 16384 | tf_op jit(solution)/shard_map/all_to_all | solution.py:373
  124.3 0.7 shard_map.115
Async XLA Ops:
  0.0 19.9 %copy-start.2 = (s32[32,8]{0,1:T(8,128)S(1)}, s32[32,8]{0,1:T(8,128)}, u32[]{:S(2)}) copy-start(s32[32,8]{0,1:T(8,128)} %param.13) | copy-start | bytes 3076
  15.9 27.2 %copy-start.3 = (f32[256]{0:T(256)S(1)}, f32[256]{0:T(256)}, u32[]{:S(2)}) copy-start(f32[256]{0:T(256)} %param.12) | copy-start | bytes 3076
  17.6 25.6 %collective-permute-start = (bf16[552,1024]{1,0:T(8,128)(2,1)S(1)}, bf16[552,1024]{1,0:T(8,128)(2,1)S(1)}, u32[]{:S(2)}, u32[]{:S(2)}) collective-permute-start(bf16[552,1024]{1,0:T(8,128)(2,1)S(1)} %get-tuple-element.13.near_ref), channel_id=1, source_target_pairs={{0,1},{1,0},{2,3},{3,2},{4,5},{5,4},{6,7},{7,6},{8,9},{9,8},{10,11... | collective-permute-start | bytes 3391496 | tf_op jit(solution)/shard_map/ppermute | solution.py:337
  72.2 21.2 %copy-start = (bf16[1,1024,256]{2,1,0:T(8,128)(2,1)S(1)}, bf16[1,1024,256]{2,1,0:T(8,128)(2,1)}, u32[]{:S(2)}) copy-start(bf16[1,1024,256]{2,1,0:T(8,128)(2,1)} %param.17) | copy-start | bytes 1572868
  72.2 21.2 %copy-start.1 = (bf16[1024,256]{1,0:T(8,128)(2,1)S(1)}, bf16[1024,256]{1,0:T(8,128)(2,1)}, u32[]{:S(2)}) copy-start(bf16[1024,256]{1,0:T(8,128)(2,1)} %shared_down_ref.1) | copy-start | bytes 1572868

commit v5 on v4

--- a/solution.py
+++ b/solution.py
@@ -69,19 +69,18 @@
     ).astype(bf16)
 
 
-def combine_weights(routes_ref, weights_ref, out_ref):
+def combine_weights(core, routes_ref, weights_ref, out_ref):
     routes, given = routes_ref[...].T, weights_ref[...].T
     named, rank, expert, line = named_slots(routes, out_ref.shape[1])
     weight = jnp.zeros(named.shape, f32)
     for k in range(routes.shape[1]):
         weight = jnp.where(routes[:, k : k + 1] == expert, given[:, k : k + 1], weight)
-    slot = 3 * ((line >> 1) & 1) + (line >> 2)
-    weight = jnp.where(named & (rank == slot), weight, 0.0)
+    weight = jnp.where(named & (rank == 3 * core + (line >> 2)), weight, 0.0)
     rows = weight.shape[0]
     at = 0
     for part in three_parts(weight):
-        for side in range(2):
-            out_ref[at : at + rows] = jnp.where((line & 1) == side, part, 0.0).astype(bf16)
+        for quarter in range(4):
+            out_ref[at : at + rows] = jnp.where((line & 3) == quarter, part, 0.0).astype(bf16)
             at += rows
 
 
@@ -97,7 +96,6 @@
     weights_ref,
     out_gain_ref,
     swap_ref,
-    keep_ref,
     combine_ref,
     later_gain_ref,
     own_gain,
@@ -125,7 +123,7 @@
     first = core == 0
     for copy in copies[:3]:
         copy.wait()
-    combine_weights(routes, weights, combine_ref)
+    combine_weights(core, routes, weights, combine_ref)
     gain = own_gain[...]
     rows = (both_ref[core].astype(f32) * gain).astype(bf16)
     half = rows.shape[0] // 2
@@ -133,17 +131,19 @@
     line = iota((8, gain.shape[1]), 0)
     gain = jnp.where(line == 0, parts[0], jnp.where(line == 1, parts[1], parts[2]))
     gain = jnp.where(line < 3, gain, 0.0).astype(bf16)
-    swap_ref[2 * depth + 2 * half :] = jnp.concatenate([gain] * 4, axis=1)
+    gain_at = 2 * depth + 2 * half
+    kept_at = gain_at + 8
+    swap_ref[gain_at:kept_at] = jnp.concatenate([gain] * 4, axis=1)
     for copy in copies[3:5]:
         copy.wait()
-    for n in range(keep_ref.shape[0]):
+    for n in range(8):
         cut = slice(n * 128, (n + 1) * 128)
         part = dot(rows, jnp.concatenate([shared_gate[:, cut], shared_up[:, cut]], axis=1))
-        keep_ref[n] = jnp.where(first, part[:half], part[half:])
-        at, lane = 2 * depth + n // 4 * half, n % 4 * 256
-        swap_ref[at : at + half, lane : lane + 256] = jnp.where(
-            first, part[half:], part[:half]
-        ).astype(bf16)
+        low, high = part[:half].astype(bf16), part[half:].astype(bf16)
+        lanes = slice(n % 4 * 256, n % 4 * 256 + 256)
+        at = n // 4 * half
+        swap_ref[2 * depth + at : 2 * depth + at + half, lanes] = jnp.where(first, high, low)
+        swap_ref[kept_at + at : kept_at + at + half, lanes] = jnp.where(first, low, high)
     for copy in copies[5:]:
         copy.wait()
 
@@ -155,7 +155,6 @@
     gain_ref,
     near_ref,
     far_ref,
-    kept_ref,
     out_ref,
     wide,
 ):
@@ -179,7 +178,8 @@
     own = (own * gain_ref[...]).astype(bf16)
     depth = gain_ref.shape[1]
     shared_at = 2 * depth
-    swapped = far_ref[shared_at + 2 * half :, :depth].astype(f32)
+    kept_at = shared_at + 2 * half + 8
+    swapped = far_ref[kept_at - 8 : kept_at, :depth].astype(f32)
     gain_other = swapped[0:1] + swapped[1:2] + swapped[2:3]
     other = (other * gain_other).astype(bf16)
     for n in range(out_ref.shape[0]):
@@ -187,14 +187,15 @@
         near = jnp.concatenate([near_ref[:depth, cut], near_ref[depth:shared_at, cut]], axis=1)
         far = jnp.concatenate([far_ref[:depth, cut], far_ref[depth:shared_at, cut]], axis=1)
         out_ref[n, :slots] = (dot(own, near) + dot(other, far)).astype(bf16)
-        at, lane = shared_at + n // 4 * half, n % 4 * 256
-        given = far_ref[at : at + half, lane : lane + 256].astype(f32)
-        out_ref[n, slots : slots + half] = (kept_ref[n] + given).astype(bf16)
+        at, lanes = n // 4 * half, slice(n % 4 * 256, n % 4 * 256 + 256)
+        given = far_ref[shared_at + at : shared_at + at + half, lanes].astype(f32)
+        kept = near_ref[kept_at + at : kept_at + at + half, lanes].astype(f32)
+        out_ref[n, slots : slots + half] = (kept + given).astype(bf16)
         out_ref[n, slots + half :] = extra
 
 
 def hidden_kernel(parts_ref, out_ref):
-    rows = out_ref.shape[0]
+    rows = out_ref.shape[1]
     total = parts_ref[0].astype(f32)
     for n in range(1, parts_ref.shape[0]):
         total = total + parts_ref[n].astype(f32)
@@ -202,38 +203,45 @@
     scale = to_column(lax.rsqrt(mean + EPS), rows)
     gate = jnp.where(scale > 0.0, total[:rows, :128] * scale, 0.0)
     up = jnp.where(scale > 0.0, total[:rows, 128:] * scale, 0.0)
-    out_ref[...] = (gate / (1.0 + jnp.exp(-gate)) * up).astype(bf16)
-
-
-def lanes_of(ref, core, lo, hi):
-    return jnp.concatenate([ref[n, lo:hi] for n in range(core, ref.shape[0], 2)], axis=1)
-
-
-def down_kernel(hidden_ref, down_ref, shared_down_ref, out_ref, shared_ref, wide):
+    hidden = (gate / (1.0 + jnp.exp(-gate)) * up).astype(bf16)
+    for n in range(out_ref.shape[0]):
+        out_ref[n] = hidden
+
+
+def down_kernel(
+    hidden_ref, near_ref, far_ref, near_shared_ref, far_shared_ref, out_ref, shared_ref, wide
+):
     slots = out_ref.shape[0] // 4
-    down = down_ref[...]
-    for core in range(2):
-        rows = dot(lanes_of(hidden_ref, core, 0, slots), down)
+    hidden = jnp.concatenate([hidden_ref[n] for n in range(hidden_ref.shape[0])], axis=1)
+    shared_refs = (near_shared_ref, far_shared_ref)
+    for n, down_ref in enumerate((near_ref, far_ref)):
+        rows = dot(hidden[:slots], down_ref[...])
         for side in range(2):
-            wide[pl.ds(2 * core + side, slots, stride=4), :] = rows[
+            wide[pl.ds(2 * n + side, slots, stride=4), :] = rows[
                 :, side * 128 : (side + 1) * 128
             ]
+        shared_ref[n] = dot(hidden[slots:], shared_refs[n][...])
     out_ref[...] = wide[...].astype(bf16)
-    end = hidden_ref.shape[1]
-    hidden = jnp.concatenate(
-        [lanes_of(hidden_ref, core, slots, end) for core in range(2)], axis=0
-    )
-    shared_ref[...] = dot(hidden, shared_down_ref[...])
-
-
-def combine_kernel(rows_ref, weights_ref, shared_ref, gain_ref, mixed_ref, squares_ref):
+
+
+def combine_kernel(core_ref, rows_ref, weights_ref, shared_ref, near_ref, far_ref):
+    first = core_ref[0] == 0
     parts = dot(weights_ref[...], rows_ref[...])
-    count = shared_ref.shape[0]
-    low, high = (
-        sum(parts[at * count : (at + 1) * count] for at in (side, side + 2, side + 4))
-        for side in range(2)
-    )
-    mixed = shared_ref[...] + jnp.concatenate([low, high], axis=1)
+    count = near_ref.shape[0]
+    quarter = [
+        sum(parts[at * count : (at + 1) * count] for at in (n, n + 4, n + 8)) for n in range(4)
+    ]
+    for n, out_ref in enumerate((near_ref, far_ref)):
+        shared = shared_ref[n]
+        none = jnp.zeros_like(shared)
+        low, high = jnp.where(first, shared, none), jnp.where(first, none, shared)
+        out_ref[...] = jnp.concatenate(quarter[2 * n : 2 * n + 2], axis=1) + jnp.concatenate(
+            [low, high], axis=0
+        )
+
+
+def mix_kernel(core_ref, near_ref, both_ref, gain_ref, mixed_ref, squares_ref):
+    mixed = near_ref[...] + both_ref[1 - core_ref[0]]
     mixed_ref[...] = mixed * gain_ref[...]
     squares = to_row(jnp.sum(mixed * mixed, axis=1, keepdims=True), 128)
     squares_ref[...] = jnp.broadcast_to(squares[None], squares_ref.shape)
@@ -305,12 +313,11 @@
     both = lax.all_gather(tokens, "core", axis=0)
     outgoing = call(pack_kernel, shape((sent, 128), bf16), core, routes, both)
     arrived = exchanged(outgoing, sources)
-    near, kept, weights, later_gain = call(
+    near, weights, later_gain = call(
         swap_kernel,
         (
-            shape((2 * features + 2 * half + 8, 1024), bf16),
-            shape((lines, half, 256), f32),
-            shape((6 * rows, sent), bf16),
+            shape((2 * features + 4 * half + 8, 1024), bf16),
+            shape((12 * rows, sent), bf16),
             shape((1, features), f32),
         ),
         core,
@@ -335,6 +342,9 @@
         ],
     )
     far = lax.ppermute(near, "core", swap)
+    far_down = lax.ppermute(down, "core", swap)
+    far_shared = lax.ppermute(shared_down, "core", swap)
+    far, far_down, far_shared = lax.optimization_barrier((far, far_down, far_shared))
 
     parts = call(
         hidden_parts_kernel,
@@ -345,29 +355,39 @@
         gain,
         near,
         far,
-        kept,
         flops=4 * slots * features * 2048,
         scratch=[pltpu.VMEM((sent, 128), f32)],
     )
     parts = lax.all_to_all(parts, "x", 0, 0, tiled=True)
-    hidden = call(hidden_kernel, shape((slots + half, 128), bf16), parts)
-    hidden = lax.all_gather(hidden, ("x", "core"), axis=0)
+    hidden = call(hidden_kernel, shape((lines, slots + half, 128), bf16), parts)
+    hidden = lax.all_to_all(hidden, "x", 0, 0, tiled=True)
     leaving, shared = call(
         down_kernel,
-        (shape((sent, 128), bf16), shape((rows, features), f32)),
+        (shape((sent, 128), bf16), shape((2, half, features), f32)),
         hidden,
         down,
+        far_down,
         shared_down,
+        far_shared,
         scratch=[pltpu.VMEM((sent, 128), f32)],
         flops=4 * slots * 1024 * features,
     )
     returned = exchanged(leaving, sources)
-    mixed, squares = call(
+    near_mixed, far_mixed = call(
         combine_kernel,
-        (shape((rows, features), f32), shape((lines * cores, 1, 128), f32)),
+        (shape((rows, features), f32), shape((rows, features), f32)),
+        core,
         returned,
         weights,
         shared,
+    )
+    far_mixed = lax.all_gather(far_mixed, "core", axis=0)
+    mixed, squares = call(
+        mix_kernel,
+        (shape((rows, features), f32), shape((lines * cores, 1, 128), f32)),
+        core,
+        near_mixed,
+        far_mixed,
         later_gain,
     )
     squares = lax.all_to_all(squares, ("x", "core"), 0, 0, tiled=True)

time: 125 us -> 131 us (1.048)
  blocking collectives: 118 us -> 94.5 us
  starting transfers between devices: 2.26 us -> 17.1 us
  waiting for transfers between devices: 0.01 us -> 12.3 us
  Pallas kernels: 4.53 us -> 6.9 us
    all_to_all x2 -> x1, blocking collectives: 39.7 us -> 20.4 us  [exchanged(): return lax.all_to_all(blocks, 'ep', 0, 0, tiled=True).reshape(rows.shape)]
    all_gather x1, blocking collectives: 21 us -> 6.39 us  [per_device(): far_mixed = lax.all_gather(far_mixed, 'core', axis=0)]
    all_to_all x0 -> x1, blocking collectives: none -> 13.5 us  [per_device(): hidden = lax.all_to_all(hidden, 'x', 0, 0, tiled=True)]
    all_to_all x0 -> x1, waiting for transfers between devices: none -> 12.3 us  [exchanged(): return lax.all_to_all(blocks, 'ep', 0, 0, tiled=True).reshape(rows.shape)]
    all_to_all x0 -> x1, starting transfers between devices: none -> 10.5 us  [exchanged(): return lax.all_to_all(blocks, 'ep', 0, 0, tiled=True).reshape(rows.shape)]
    ppermute x0 -> x2, starting transfers between devices: none -> 4.33 us  [the longest x1 2.26 us: per_device(): far_shared = lax.ppermute(shared_down, 'core', swap)]
    all_to_all x1, blocking collectives: 13 us -> 9.83 us  [per_device(): squares = lax.all_to_all(squares, ('x', 'core'), 0, 0, tiled=True)]
    pallas_call x7 -> x8, Pallas kernels: 4.53 us -> 6.9 us  [call(): pl.pallas_call(body, out_shape=out, in_specs=[spec(n, a) for n, a in enum...]
  transfers between devices with their start and end apart: 1 -> 4, of which waited for: 0 -> 1; matrix products, arithmetic and copies ran while one was open for 0% -> 0% of each run, Pallas kernels for 0% -> 1%
where the time goes in v5:
time: 131 us
  blocking collectives  94.5 us (72%)
  starting transfers between devices  17.1 us (13%)
  waiting for transfers between devices  12.3 us (9%)
  Pallas kernels  6.9 us (5%)
    all_to_all x1, blocking collectives, per_device(): parts = lax.all_to_all(parts, 'x', 0, 0, tiled=True)  28.5 us
    all_to_all x1, blocking collectives, exchanged(): return lax.all_to_all(blocks, 'ep', 0, 0, tiled=True).reshape(rows.shape)  20.4 us
    all_gather x1, blocking collectives, per_device(): both = lax.all_gather(tokens, 'core', axis=0)  15.9 us
    all_to_all x1, blocking collectives, per_device(): hidden = lax.all_to_all(hidden, 'x', 0, 0, tiled=True)  13.5 us
    all_to_all x1, waiting for transfers between devices, exchanged(): return lax.all_to_all(blocks, 'ep', 0, 0, tiled=True).reshape(rows.shape)  12.3 us
    all_to_all x1, starting transfers between devices, exchanged(): return lax.all_to_all(blocks, 'ep', 0, 0, tiled=True).reshape(rows.shape)  10.5 us
    all_to_all x1, blocking collectives, per_device(): squares = lax.all_to_all(squares, ('x', 'core'), 0, 0, tiled=True)  9.83 us
    pallas_call x8, Pallas kernels, call(): pl.pallas_call(body, out_shape=out, in_specs=[spec(n, a) for n, a in enum...  6.9 us
  transfers between devices with their start and end apart: 4, of which 1 were waited for; matrix products, arithmetic and copies ran while one was open for 0% of the time, Pallas kernels for 1%

profile of v5, /device:TPU:1, one launch (start us, length us, event | category | flops | bytes accessed | tf_op | source)
XLA Modules:
  0.0 131.0 jit_solution(14935838427534386695)
XLA Ops:
  0.0 0.0 copy-start
  0.0 15.9 %all-gather = bf16[64,256]{1,0:T(8,128)(2,1)S(1)} all-gather(bf16[32,256]{1,0:T(8,128)(2,1)} %param.11), channel_id=2, replica_groups=mesh['ep'=64,'x'=8,'core'=2] {'core'}, dimensions={0}, use_global_device_ids=true | all-gather | bytes 49152 | tf_op jit(solution)/shard_map/all_gather | solution.py:313
  15.9 0.0 copy-start.1
  15.9 1.7 %shard_map.110 = (bf16[584,1024]{1,0:T(8,128)(2,1)S(1)}, bf16[384,768]{1,0:T(8,128)(2,1)S(1)}, f32[1,256]{1,0:T(1,128)S(1)}) custom-call(s32[1]{0:T(128)} %bitcast.core_ref, bf16[2,32,256]{2,1,0:T(8,128)(2,1)S(1)} %bitcast.16, f32[1,256]{1,0:T(1,128)} %bitcast.23, bf16[256,1024]{1,0:T(8,128)(2,1)} %bitcast.25, bf16[256,1024]{1,0:T(8,128)(2,1)} %bitcast.26, ...), custom_call_target="tpu_custom_call" | custom-call | flops 33554432 | bytes 3920900 | tf_op jit(solution)/shard_map/pallas_call | solution.py:269
  17.6 2.3 %collective-permute-start = (bf16[584,1024]{1,0:T(8,128)(2,1)S(1)}, bf16[584,1024]{1,0:T(8,128)(2,1)S(1)}, u32[]{:S(2)}, u32[]{:S(2)}) collective-permute-start(bf16[584,1024]{1,0:T(8,128)(2,1)S(1)} %get-tuple-element.17.near_ref), channel_id=1, source_target_pairs={{0,1},{1,0},{2,3},{3,2},{4,5},{5,4},{6,7},{7,6},{8,9},{9,8},{10,11... | collective-permute-start | bytes 3588104 | tf_op jit(solution)/shard_map/ppermute | solution.py:344
  19.9 2.1 %collective-permute-start.1 = (bf16[1024,256]{1,0:T(8,128)(2,1)}, bf16[1024,256]{1,0:T(8,128)(2,1)}, u32[]{:S(2)}, u32[]{:S(2)}) collective-permute-start(bf16[1024,256]{1,0:T(8,128)(2,1)} %bitcast.10.near_ref), channel_id=1, source_target_pairs={{0,1},{1,0},{2,3},{3,2},{4,5},{5,4},{6,7},{7,6},{8,9},{9,8},{10,11... | collective-permute-start | bytes 1572872 | tf_op jit(solution)/shard_map/ppermute | solution.py:345
  21.9 2.3 %collective-permute-start.2 = (bf16[1024,256]{1,0:T(8,128)(2,1)}, bf16[1024,256]{1,0:T(8,128)(2,1)}, u32[]{:S(2)}, u32[]{:S(2)}) collective-permute-start(bf16[1024,256]{1,0:T(8,128)(2,1)} %near_shared_ref.1), channel_id=1, source_target_pairs={{0,1},{1,0},{2,3},{3,2},{4,5},{5,4},{6,7},{7,6},{8,9},{9,8},{10,11... | collective-permute-start | bytes 1572872 | tf_op jit(solution)/shard_map/ppermute | solution.py:346
  24.2 0.0 copy-done
  24.2 1.3 shard_map.109
  25.5 10.5 %all-to-all-start = ((bf16[64,3,4,128]{3,2,1,0:T(4,128)(2,1)}), bf16[64,3,4,128]{3,2,1,0:T(4,128)(2,1)S(1)}, u32[]{:S(2)}, u32[]{:S(2)}) async-start(bf16[64,3,4,128]{3,2,1,0:T(4,128)(2,1)} %bitcast.3), calls=%async_computation | async-start | bytes 393216 | tf_op jit(solution)/shard_map/all_to_all | solution.py:286
  36.0 0.0 collective-permute-done.1.far_ref
  36.0 0.0 collective-permute-done.2.far_shared_ref
  36.1 0.0 collective-permute-done.far_ref
  36.1 12.3 %all-to-all-done = bf16[64,3,4,128]{3,2,1,0:T(4,128)(2,1)S(1)} async-done(((bf16[64,3,4,128]{3,2,1,0:T(4,128)(2,1)}), bf16[64,3,4,128]{3,2,1,0:T(4,128)(2,1)S(1)}, u32[]{:S(2)}, u32[]{:S(2)}) %all-to-all-start) | async-done | bytes 196640 | tf_op jit(solution)/shard_map/all_to_all | solution.py:286
  48.4 0.0 copy-done.1
  48.4 0.6 shard_map.111
  49.0 28.5 %all_to_all.25.parts_ref = bf16[8,216,256]{2,1,0:T(8,128)(2,1)S(1)} all-to-all(bf16[8,216,256]{2,1,0:T(8,128)(2,1)S(1)} %shard_map.111), channel_id=1, replica_groups=mesh['ep'=64,'x'=8,'core'=2] {'x'}, dimensions={0} | all-to-all | bytes 1769472 | tf_op jit(solution)/shard_map/all_to_all | solution.py:361
  77.5 0.2 shard_map.112
  77.7 13.5 %all_to_all.26.hidden_ref = bf16[8,208,128]{2,1,0:T(8,128)(2,1)S(1)} all-to-all(bf16[8,208,128]{2,1,0:T(8,128)(2,1)S(1)} %shard_map.112), channel_id=1, replica_groups=mesh['ep'=64,'x'=8,'core'=2] {'x'}, dimensions={0} | all-to-all | bytes 851968 | tf_op jit(solution)/shard_map/all_to_all | solution.py:363
  91.2 2.0 %shard_map.113 = (bf16[768,128]{1,0:T(8,128)(2,1)S(1)}, f32[2,16,256]{2,1,0:T(8,128)S(1)}) custom-call(bf16[8,208,128]{2,1,0:T(8,128)(2,1)S(1)} %all_to_all.26.hidden_ref, bf16[1024,256]{1,0:T(8,128)(2,1)} %bitcast.10.near_ref, bf16[1024,256]{1,0:T(8,128)(2,1)} %collective-permute-done.1.far_ref, bf16[1024,256]{1,0:T(8,128)(2,1)} %near_shared_ref.1, ...), custom_call_target="tpu_custom_call" | custom-call | flops 201326592 | bytes 2752512 | tf_op jit(solution)/shard_map/pallas_call | solution.py:269
  93.2 20.4 %all_to_all.27 = bf16[64,3,4,128]{3,2,1,0:T(4,128)(2,1)S(1)} all-to-all(bf16[64,3,4,128]{3,2,1,0:T(4,128)(2,1)S(1)} %bitcast.20), channel_id=1, replica_groups=mesh['ep'=64,'x'=8,'core'=2] {'ep'}, dimensions={0} | all-to-all | bytes 393216 | tf_op jit(solution)/shard_map/all_to_all | solution.py:286
  113.6 0.3 shard_map.114
  114.0 6.4 %all-gather.1 = f32[64,256]{1,0:T(8,128)S(1)} all-gather(f32[32,256]{1,0:T(8,128)S(1)} %get-tuple-element.25), channel_id=3, replica_groups=mesh['ep'=64,'x'=8,'core'=2] {'core'}, dimensions={0}, use_global_device_ids=true | all-gather | bytes 98304 | tf_op jit(solution)/shard_map/all_gather | solution.py:384
  120.4 0.1 shard_map.115
  120.5 9.8 %all_to_all.28.squares_ref = f32[16,1,128]{2,1,0:T(1,128)S(1)} all-to-all(f32[16,1,128]{2,1,0:T(1,128)S(1)} %get-tuple-element.27), channel_id=1, replica_groups=mesh['ep'=64,'x'=8,'core'=2] {'x','core'}, dimensions={0} | all-to-all | bytes 16384 | tf_op jit(solution)/shard_map/all_to_all | solution.py:393
  130.3 0.7 shard_map.116
Async XLA Ops:
  0.0 24.2 %copy-start = (s32[32,8]{0,1:T(8,128)S(1)}, s32[32,8]{0,1:T(8,128)}, u32[]{:S(2)}) copy-start(s32[32,8]{0,1:T(8,128)} %param.13) | copy-start | bytes 3076
  15.9 32.5 %copy-start.1 = (f32[256]{0:T(256)S(1)}, f32[256]{0:T(256)}, u32[]{:S(2)}) copy-start(f32[256]{0:T(256)} %param.12) | copy-start | bytes 3076
  17.6 18.5 %collective-permute-start = (bf16[584,1024]{1,0:T(8,128)(2,1)S(1)}, bf16[584,1024]{1,0:T(8,128)(2,1)S(1)}, u32[]{:S(2)}, u32[]{:S(2)}) collective-permute-start(bf16[584,1024]{1,0:T(8,128)(2,1)S(1)} %get-tuple-element.17.near_ref), channel_id=1, source_target_pairs={{0,1},{1,0},{2,3},{3,2},{4,5},{5,4},{6,7},{7,6},{8,9},{9,8},{10,11... | collective-permute-start | bytes 3588104 | tf_op jit(solution)/shard_map/ppermute | solution.py:344
  19.9 16.2 %collective-permute-start.1 = (bf16[1024,256]{1,0:T(8,128)(2,1)}, bf16[1024,256]{1,0:T(8,128)(2,1)}, u32[]{:S(2)}, u32[]{:S(2)}) collective-permute-start(bf16[1024,256]{1,0:T(8,128)(2,1)} %bitcast.10.near_ref), channel_id=1, source_target_pairs={{0,1},{1,0},{2,3},{3,2},{4,5},{5,4},{6,7},{7,6},{8,9},{9,8},{10,11... | collective-permute-start | bytes 1572872 | tf_op jit(solution)/shard_map/ppermute | solution.py:345
  21.9 14.1 %collective-permute-start.2 = (bf16[1024,256]{1,0:T(8,128)(2,1)}, bf16[1024,256]{1,0:T(8,128)(2,1)}, u32[]{:S(2)}, u32[]{:S(2)}) collective-permute-start(bf16[1024,256]{1,0:T(8,128)(2,1)} %near_shared_ref.1), channel_id=1, source_target_pairs={{0,1},{1,0},{2,3},{3,2},{4,5},{5,4},{6,7},{7,6},{8,9},{9,8},{10,11... | collective-permute-start | bytes 1572872 | tf_op jit(solution)/shard_map/ppermute | solution.py:346
  25.5 22.9 %all-to-all-start = ((bf16[64,3,4,128]{3,2,1,0:T(4,128)(2,1)}), bf16[64,3,4,128]{3,2,1,0:T(4,128)(2,1)S(1)}, u32[]{:S(2)}, u32[]{:S(2)}) async-start(bf16[64,3,4,128]{3,2,1,0:T(4,128)(2,1)} %bitcast.3), calls=%async_computation | async-start | bytes 393216 | tf_op jit(solution)/shard_map/all_to_all | solution.py:286

commit v6 on v4

--- a/solution.py
+++ b/solution.py
@@ -194,7 +194,7 @@
 
 
 def hidden_kernel(parts_ref, out_ref):
-    rows = out_ref.shape[0]
+    rows = out_ref.shape[1]
     total = parts_ref[0].astype(f32)
     for n in range(1, parts_ref.shape[0]):
         total = total + parts_ref[n].astype(f32)
@@ -202,11 +202,13 @@
     scale = to_column(lax.rsqrt(mean + EPS), rows)
     gate = jnp.where(scale > 0.0, total[:rows, :128] * scale, 0.0)
     up = jnp.where(scale > 0.0, total[:rows, 128:] * scale, 0.0)
-    out_ref[...] = (gate / (1.0 + jnp.exp(-gate)) * up).astype(bf16)
+    hidden = (gate / (1.0 + jnp.exp(-gate)) * up).astype(bf16)
+    for n in range(out_ref.shape[0]):
+        out_ref[n] = hidden
 
 
 def lanes_of(ref, core, lo, hi):
-    return jnp.concatenate([ref[n, lo:hi] for n in range(core, ref.shape[0], 2)], axis=1)
+    return jnp.concatenate([ref[core, n, lo:hi] for n in range(ref.shape[1])], axis=1)
 
 
 def down_kernel(hidden_ref, down_ref, shared_down_ref, out_ref, shared_ref, wide):
@@ -219,7 +221,7 @@
                 :, side * 128 : (side + 1) * 128
             ]
     out_ref[...] = wide[...].astype(bf16)
-    end = hidden_ref.shape[1]
+    end = hidden_ref.shape[2]
     hidden = jnp.concatenate(
         [lanes_of(hidden_ref, core, slots, end) for core in range(2)], axis=0
     )
@@ -350,8 +352,9 @@
         scratch=[pltpu.VMEM((sent, 128), f32)],
     )
     parts = lax.all_to_all(parts, "x", 0, 0, tiled=True)
-    hidden = call(hidden_kernel, shape((slots + half, 128), bf16), parts)
-    hidden = lax.all_gather(hidden, ("x", "core"), axis=0)
+    hidden = call(hidden_kernel, shape((lines, slots + half, 128), bf16), parts)
+    hidden = lax.all_to_all(hidden, "x", 0, 0, tiled=True)
+    hidden = lax.all_gather(hidden, "core", axis=0)
     leaving, shared = call(
         down_kernel,
         (shape((sent, 128), bf16), shape((rows, features), f32)),

time: 125 us -> 126 us (level)
    all_to_all x0 -> x1, blocking collectives: none -> 13.7 us  [per_device(): hidden = lax.all_to_all(hidden, 'x', 0, 0, tiled=True)]
    all_gather x1, blocking collectives: 21 us -> 7.36 us  [per_device(): hidden = lax.all_gather(hidden, 'core', axis=0)]
    all_to_all x2, blocking collectives: 39.7 us -> 41.4 us  [exchanged(): return lax.all_to_all(blocks, 'ep', 0, 0, tiled=True).reshape(rows.shape)]
where the time goes in v6:
time: 126 us
  blocking collectives  119 us (94%)
  Pallas kernels  4.53 us (4%)
  starting transfers between devices  2.26 us (2%)
    all_to_all x2, blocking collectives, exchanged(): return lax.all_to_all(blocks, 'ep', 0, 0, tiled=True).reshape(rows.shape)  41.4 us
    all_to_all x1, blocking collectives, per_device(): parts = lax.all_to_all(parts, 'x', 0, 0, tiled=True)  28.5 us
    all_gather x1, blocking collectives, per_device(): both = lax.all_gather(tokens, 'core', axis=0)  15.9 us
    all_to_all x1, blocking collectives, per_device(): hidden = lax.all_to_all(hidden, 'x', 0, 0, tiled=True)  13.7 us
    all_to_all x1, blocking collectives, per_device(): squares = lax.all_to_all(squares, ('x', 'core'), 0, 0, tiled=True)  12 us
    all_gather x1, blocking collectives, per_device(): hidden = lax.all_gather(hidden, 'core', axis=0)  7.36 us
    pallas_call x7, Pallas kernels, call(): pl.pallas_call(body, out_shape=out, in_specs=[spec(n, a) for n, a in enum...  4.53 us
  transfers between devices with their start and end apart: 1, of which 0 were waited for; matrix products, arithmetic and copies ran while one was open for 0% of the time, Pallas kernels for 0%

profile of v6, /device:TPU:1, one launch (start us, length us, event | category | flops | bytes accessed | tf_op | source)
XLA Modules:
  0.0 125.7 jit_solution(16506757317637277240)
XLA Ops:
  0.0 0.0 copy-start.2
  0.0 15.9 %all-gather = bf16[64,256]{1,0:T(8,128)(2,1)S(1)} all-gather(bf16[32,256]{1,0:T(8,128)(2,1)} %param.11), channel_id=2, replica_groups=mesh['ep'=64,'x'=8,'core'=2] {'core'}, dimensions={0}, use_global_device_ids=true | all-gather | bytes 49152 | tf_op jit(solution)/shard_map/all_gather | solution.py:307
  15.9 0.0 copy-start.3
  15.9 1.7 %shard_map.110 = (bf16[552,1024]{1,0:T(8,128)(2,1)S(1)}, f32[8,16,256]{2,1,0:T(8,128)S(1)}, bf16[192,768]{1,0:T(8,128)(2,1)S(1)}, f32[1,256]{1,0:T(1,128)S(1)}) custom-call(s32[1]{0:T(128)} %bitcast.core_ref, bf16[2,32,256]{2,1,0:T(8,128)(2,1)S(1)} %bitcast.18, f32[1,256]{1,0:T(1,128)} %bitcast.25, bf16[256,1024]{1,0:T(8,128)(2,1)} %bitcast.27, ...), custom_call_target="tpu_custom_call" | custom-call | flops 33554432 | bytes 3691524 | tf_op jit(solution)/shard_map/pallas_call | solution.py:263
  17.6 2.3 %collective-permute-start = (bf16[552,1024]{1,0:T(8,128)(2,1)S(1)}, bf16[552,1024]{1,0:T(8,128)(2,1)S(1)}, u32[]{:S(2)}, u32[]{:S(2)}) collective-permute-start(bf16[552,1024]{1,0:T(8,128)(2,1)S(1)} %get-tuple-element.13.near_ref), channel_id=1, source_target_pairs={{0,1},{1,0},{2,3},{3,2},{4,5},{5,4},{6,7},{7,6},{8,9},{9,8},{10,11... | collective-permute-start | bytes 3391496 | tf_op jit(solution)/shard_map/ppermute | solution.py:339
  19.9 0.0 copy-done.2
  19.9 0.6 shard_map.109
  20.5 22.7 %all_to_all.25 = bf16[64,3,4,128]{3,2,1,0:T(4,128)(2,1)S(1)} all-to-all(bf16[64,3,4,128]{3,2,1,0:T(4,128)(2,1)S(1)} %bitcast.16), channel_id=1, replica_groups=mesh['ep'=64,'x'=8,'core'=2] {'ep'}, dimensions={0} | all-to-all | bytes 393216 | tf_op jit(solution)/shard_map/all_to_all | solution.py:280
  43.2 0.0 collective-permute-done.far_ref
  43.2 0.0 copy-done.3
  43.2 0.6 shard_map.111
  43.8 28.5 %all_to_all.26.parts_ref = bf16[8,216,256]{2,1,0:T(8,128)(2,1)S(1)} all-to-all(bf16[8,216,256]{2,1,0:T(8,128)(2,1)S(1)} %shard_map.111), channel_id=1, replica_groups=mesh['ep'=64,'x'=8,'core'=2] {'x'}, dimensions={0} | all-to-all | bytes 1769472 | tf_op jit(solution)/shard_map/all_to_all | solution.py:354
  72.2 0.2 shard_map.112
  72.4 0.0 copy-start
  72.4 0.0 copy-start.1
  72.5 13.7 %all_to_all.27 = bf16[8,208,128]{2,1,0:T(8,128)(2,1)S(1)} all-to-all(bf16[8,208,128]{2,1,0:T(8,128)(2,1)S(1)} %shard_map.112), channel_id=1, replica_groups=mesh['ep'=64,'x'=8,'core'=2] {'x'}, dimensions={0} | all-to-all | bytes 851968 | tf_op jit(solution)/shard_map/all_to_all | solution.py:356
  86.1 7.4 %all-gather.1 = bf16[16,208,128]{2,1,0:T(8,128)(2,1)S(1)} all-gather(bf16[8,208,128]{2,1,0:T(8,128)(2,1)S(1)} %all_to_all.27), channel_id=3, replica_groups=mesh['ep'=64,'x'=8,'core'=2] {'core'}, dimensions={0}, use_global_device_ids=true | all-gather | bytes 1277952 | tf_op jit(solution)/shard_map/all_gather | solution.py:357
  93.5 0.0 copy-done
  93.5 0.0 copy-done.1
  93.5 0.5 shard_map.113
  93.9 18.7 %all_to_all.28 = bf16[64,3,4,128]{3,2,1,0:T(4,128)(2,1)S(1)} all-to-all(bf16[64,3,4,128]{3,2,1,0:T(4,128)(2,1)S(1)} %bitcast.22), channel_id=1, replica_groups=mesh['ep'=64,'x'=8,'core'=2] {'ep'}, dimensions={0} | all-to-all | bytes 393216 | tf_op jit(solution)/shard_map/all_to_all | solution.py:280
  112.7 0.3 shard_map.114
  113.0 12.0 %all_to_all.29.squares_ref = f32[16,1,128]{2,1,0:T(1,128)S(1)} all-to-all(f32[16,1,128]{2,1,0:T(1,128)S(1)} %get-tuple-element.19), channel_id=1, replica_groups=mesh['ep'=64,'x'=8,'core'=2] {'x','core'}, dimensions={0} | all-to-all | bytes 16384 | tf_op jit(solution)/shard_map/all_to_all | solution.py:376
  125.0 0.7 shard_map.115
Async XLA Ops:
  0.0 19.9 %copy-start.2 = (s32[32,8]{0,1:T(8,128)S(1)}, s32[32,8]{0,1:T(8,128)}, u32[]{:S(2)}) copy-start(s32[32,8]{0,1:T(8,128)} %param.13) | copy-start | bytes 3076
  15.9 27.2 %copy-start.3 = (f32[256]{0:T(256)S(1)}, f32[256]{0:T(256)}, u32[]{:S(2)}) copy-start(f32[256]{0:T(256)} %param.12) | copy-start | bytes 3076
  17.6 25.6 %collective-permute-start = (bf16[552,1024]{1,0:T(8,128)(2,1)S(1)}, bf16[552,1024]{1,0:T(8,128)(2,1)S(1)}, u32[]{:S(2)}, u32[]{:S(2)}) collective-permute-start(bf16[552,1024]{1,0:T(8,128)(2,1)S(1)} %get-tuple-element.13.near_ref), channel_id=1, source_target_pairs={{0,1},{1,0},{2,3},{3,2},{4,5},{5,4},{6,7},{7,6},{8,9},{9,8},{10,11... | collective-permute-start | bytes 3391496 | tf_op jit(solution)/shard_map/ppermute | solution.py:339
  72.4 21.1 %copy-start = (bf16[1,1024,256]{2,1,0:T(8,128)(2,1)S(1)}, bf16[1,1024,256]{2,1,0:T(8,128)(2,1)}, u32[]{:S(2)}) copy-start(bf16[1,1024,256]{2,1,0:T(8,128)(2,1)} %param.17) | copy-start | bytes 1572868
  72.4 21.0 %copy-start.1 = (bf16[1024,256]{1,0:T(8,128)(2,1)S(1)}, bf16[1024,256]{1,0:T(8,128)(2,1)}, u32[]{:S(2)}) copy-start(bf16[1024,256]{1,0:T(8,128)(2,1)} %shared_down_ref.1) | copy-start | bytes 1572868

commit v7 on v4

--- a/solution.py
+++ b/solution.py
@@ -56,9 +56,12 @@
     return own[:, :128], own[:, 128:], other[:, :128], other[:, 128:]
 
 
-def pack_kernel(core_ref, routes_ref, both_ref, out_ref):
+def pack_kernel(core_ref, routes_ref, both_ref, out_ref, routes, sem):
+    copy = pltpu.make_async_copy(routes_ref, routes, sem)
+    copy.start()
     core = core_ref[0]
-    named, rank, _, line = named_slots(routes_ref[...].T, out_ref.shape[0])
+    copy.wait()
+    named, rank, _, line = named_slots(routes[...].T, out_ref.shape[0])
     chosen = jnp.where(named & (rank == 3 * core + (line >> 2)), 1.0, 0.0)
     picks = jnp.concatenate(
         [jnp.where((line & 3) == q, chosen, 0.0).astype(bf16) for q in range(4)], axis=0
@@ -226,7 +229,7 @@
     shared_ref[...] = dot(hidden, shared_down_ref[...])
 
 
-def combine_kernel(rows_ref, weights_ref, shared_ref, gain_ref, mixed_ref, squares_ref):
+def combine_kernel(rows_ref, weights_ref, shared_ref, mixed_ref, squares_ref):
     parts = dot(weights_ref[...], rows_ref[...])
     count = shared_ref.shape[0]
     low, high = (
@@ -234,15 +237,15 @@
         for side in range(2)
     )
     mixed = shared_ref[...] + jnp.concatenate([low, high], axis=1)
-    mixed_ref[...] = mixed * gain_ref[...]
+    mixed_ref[...] = mixed
     squares = to_row(jnp.sum(mixed * mixed, axis=1, keepdims=True), 128)
     squares_ref[...] = jnp.broadcast_to(squares[None], squares_ref.shape)
 
 
-def norm_kernel(squares_ref, mixed_ref, out_ref):
+def norm_kernel(squares_ref, mixed_ref, gain_ref, out_ref):
     total = jnp.sum(squares_ref[...], axis=0)
     scale = to_column(lax.rsqrt(total / D + EPS), out_ref.shape[0])
-    out_ref[...] = (mixed_ref[...] * scale).astype(bf16)
+    out_ref[...] = (mixed_ref[...] * scale * gain_ref[...]).astype(bf16)
 
 
 def call(body, out, *operands, flops=0, far=(), scratch=()):
@@ -303,7 +306,15 @@
 
     routes, route_weights = routes.T, route_weights.T
     both = lax.all_gather(tokens, "core", axis=0)
-    outgoing = call(pack_kernel, shape((sent, 128), bf16), core, routes, both)
+    outgoing = call(
+        pack_kernel,
+        shape((sent, 128), bf16),
+        core,
+        routes,
+        both,
+        far=(1,),
+        scratch=[pltpu.VMEM(routes.shape, i32), pltpu.SemaphoreType.DMA],
+    )
     arrived = exchanged(outgoing, sources)
     near, kept, weights, later_gain = call(
         swap_kernel,
@@ -368,10 +379,9 @@
         returned,
         weights,
         shared,
-        later_gain,
     )
     squares = lax.all_to_all(squares, ("x", "core"), 0, 0, tiled=True)
-    return call(norm_kernel, shape((rows, features), bf16), squares, mixed)
+    return call(norm_kernel, shape((rows, features), bf16), squares, mixed, later_gain)
 
 
 def solution(mesh):

time: 125 us -> 126 us (level)
  transfers between devices with their start and end apart: 1 -> 1, of which waited for: 0 -> 0; matrix products, arithmetic and copies ran while one was open for 0% -> 0% of each run, Pallas kernels for 0% -> 1%
where the time goes in v7:
time: 126 us
  blocking collectives  118 us (94%)
  Pallas kernels  5.23 us (4%)
  starting transfers between devices  2.26 us (2%)
    all_to_all x2, blocking collectives, exchanged(): return lax.all_to_all(blocks, 'ep', 0, 0, tiled=True).reshape(rows.shape)  39.7 us
    all_to_all x1, blocking collectives, per_device(): parts = lax.all_to_all(parts, 'x', 0, 0, tiled=True)  28.5 us
    all_gather x1, blocking collectives, per_device(): hidden = lax.all_gather(hidden, ('x', 'core'), axis=0)  21 us
    all_gather x1, blocking collectives, per_device(): both = lax.all_gather(tokens, 'core', axis=0)  15.8 us
    all_to_all x1, blocking collectives, per_device(): squares = lax.all_to_all(squares, ('x', 'core'), 0, 0, tiled=True)  13 us
    pallas_call x7, Pallas kernels, call(): pl.pallas_call(body, out_shape=out, in_specs=[spec(n, a) for n, a in enum...  5.23 us
  transfers between devices with their start and end apart: 1, of which 0 were waited for; matrix products, arithmetic and copies ran while one was open for 0% of the time, Pallas kernels for 1%

profile of v7, /device:TPU:1, one launch (start us, length us, event | category | flops | bytes accessed | tf_op | source)
XLA Modules:
  0.0 125.5 jit_solution(13403703117132388431)
XLA Ops:
  0.0 15.8 %all-gather = bf16[64,256]{1,0:T(8,128)(2,1)S(1)} all-gather(bf16[32,256]{1,0:T(8,128)(2,1)} %param.11), channel_id=2, replica_groups=mesh['ep'=64,'x'=8,'core'=2] {'core'}, dimensions={0}, use_global_device_ids=true | all-gather | bytes 49152 | tf_op jit(solution)/shard_map/all_gather | solution.py:308
  15.8 0.0 copy-start.2
  15.8 1.7 %shard_map.110 = (bf16[552,1024]{1,0:T(8,128)(2,1)S(1)}, f32[8,16,256]{2,1,0:T(8,128)S(1)}, bf16[192,768]{1,0:T(8,128)(2,1)S(1)}, f32[1,256]{1,0:T(1,128)S(1)}) custom-call(s32[1]{0:T(128)} %bitcast.core_ref, bf16[2,32,256]{2,1,0:T(8,128)(2,1)S(1)} %bitcast.18, f32[1,256]{1,0:T(1,128)} %bitcast.23, bf16[256,1024]{1,0:T(8,128)(2,1)} %bitcast.25, ...), custom_call_target="tpu_custom_call" | custom-call | flops 33554432 | bytes 3691524 | tf_op jit(solution)/shard_map/pallas_call | solution.py:264
  17.5 2.3 %collective-permute-start = (bf16[552,1024]{1,0:T(8,128)(2,1)S(1)}, bf16[552,1024]{1,0:T(8,128)(2,1)S(1)}, u32[]{:S(2)}, u32[]{:S(2)}) collective-permute-start(bf16[552,1024]{1,0:T(8,128)(2,1)S(1)} %get-tuple-element.13.near_ref), channel_id=1, source_target_pairs={{0,1},{1,0},{2,3},{3,2},{4,5},{5,4},{6,7},{7,6},{8,9},{9,8},{10,11... | collective-permute-start | bytes 3391496 | tf_op jit(solution)/shard_map/ppermute | solution.py:348
  19.7 1.3 %shard_map.109 = bf16[768,128]{1,0:T(8,128)(2,1)S(1)} custom-call(s32[1]{0:T(128)} %bitcast.core_ref, s32[8,32]{1,0:T(8,128)} %bitcast.28, bf16[2,32,256]{2,1,0:T(8,128)(2,1)S(1)} %bitcast.19), custom_call_target="tpu_custom_call" | custom-call | bytes 230404 | tf_op jit(solution)/shard_map/pallas_call | solution.py:264
  21.0 22.7 %all_to_all.20 = bf16[64,3,4,128]{3,2,1,0:T(4,128)(2,1)S(1)} all-to-all(bf16[64,3,4,128]{3,2,1,0:T(4,128)(2,1)S(1)} %bitcast.16), channel_id=1, replica_groups=mesh['ep'=64,'x'=8,'core'=2] {'ep'}, dimensions={0} | all-to-all | bytes 393216 | tf_op jit(solution)/shard_map/all_to_all | solution.py:281
  43.7 0.0 collective-permute-done.far_ref
  43.7 0.0 copy-done.2
  43.7 0.6 shard_map.111
  44.3 28.5 %all_to_all.21.parts_ref = bf16[8,216,256]{2,1,0:T(8,128)(2,1)S(1)} all-to-all(bf16[8,216,256]{2,1,0:T(8,128)(2,1)S(1)} %shard_map.111), channel_id=1, replica_groups=mesh['ep'=64,'x'=8,'core'=2] {'x'}, dimensions={0} | all-to-all | bytes 1769472 | tf_op jit(solution)/shard_map/all_to_all | solution.py:363
  72.8 0.0 copy-start
  72.8 0.0 copy-start.1
  72.8 0.2 shard_map.112
  73.0 21.0 %all-gather.1 = bf16[3328,128]{1,0:T(8,128)(2,1)S(1)} all-gather(bf16[208,128]{1,0:T(8,128)(2,1)S(1)} %shard_map.112), channel_id=3, replica_groups=mesh['ep'=64,'x'=8,'core'=2] {'x','core'}, dimensions={0}, use_global_device_ids=true | all-gather | bytes 905216 | tf_op jit(solution)/shard_map/all_gather | solution.py:365
  94.0 0.0 copy-done
  94.0 0.0 copy-done.1
  94.0 0.5 shard_map.113
  94.4 17.0 %all_to_all.22 = bf16[64,3,4,128]{3,2,1,0:T(4,128)(2,1)S(1)} all-to-all(bf16[64,3,4,128]{3,2,1,0:T(4,128)(2,1)S(1)} %bitcast.22), channel_id=1, replica_groups=mesh['ep'=64,'x'=8,'core'=2] {'ep'}, dimensions={0} | all-to-all | bytes 393216 | tf_op jit(solution)/shard_map/all_to_all | solution.py:281
  111.5 0.3 shard_map.114
  111.8 13.0 %all_to_all.23.squares_ref = f32[16,1,128]{2,1,0:T(1,128)S(1)} all-to-all(f32[16,1,128]{2,1,0:T(1,128)S(1)} %get-tuple-element.18), channel_id=1, replica_groups=mesh['ep'=64,'x'=8,'core'=2] {'x','core'}, dimensions={0} | all-to-all | bytes 16384 | tf_op jit(solution)/shard_map/all_to_all | solution.py:383
  124.8 0.7 shard_map.115
Async XLA Ops:
  15.8 27.9 %copy-start.2 = (f32[256]{0:T(256)S(1)}, f32[256]{0:T(256)}, u32[]{:S(2)}) copy-start(f32[256]{0:T(256)} %param.12) | copy-start | bytes 3076
  17.5 26.2 %collective-permute-start = (bf16[552,1024]{1,0:T(8,128)(2,1)S(1)}, bf16[552,1024]{1,0:T(8,128)(2,1)S(1)}, u32[]{:S(2)}, u32[]{:S(2)}) collective-permute-start(bf16[552,1024]{1,0:T(8,128)(2,1)S(1)} %get-tuple-element.13.near_ref), channel_id=1, source_target_pairs={{0,1},{1,0},{2,3},{3,2},{4,5},{5,4},{6,7},{7,6},{8,9},{9,8},{10,11... | collective-permute-start | bytes 3391496 | tf_op jit(solution)/shard_map/ppermute | solution.py:348
  72.8 21.2 %copy-start = (bf16[1,1024,256]{2,1,0:T(8,128)(2,1)S(1)}, bf16[1,1024,256]{2,1,0:T(8,128)(2,1)}, u32[]{:S(2)}) copy-start(bf16[1,1024,256]{2,1,0:T(8,128)(2,1)} %param.17) | copy-start | bytes 1572868
  72.8 21.2 %copy-start.1 = (bf16[1024,256]{1,0:T(8,128)(2,1)S(1)}, bf16[1024,256]{1,0:T(8,128)(2,1)}, u32[]{:S(2)}) copy-start(bf16[1024,256]{1,0:T(8,128)(2,1)} %shared_down_ref.1) | copy-start | bytes 1572868

commit v8 on v7

--- a/solution.py
+++ b/solution.py
@@ -56,18 +56,14 @@
     return own[:, :128], own[:, 128:], other[:, :128], other[:, 128:]
 
 
-def pack_kernel(core_ref, routes_ref, both_ref, out_ref, routes, sem):
-    copy = pltpu.make_async_copy(routes_ref, routes, sem)
-    copy.start()
-    core = core_ref[0]
-    copy.wait()
-    named, rank, _, line = named_slots(routes[...].T, out_ref.shape[0])
+def packed(core, routes, both_ref, lanes):
+    named, rank, _, line = named_slots(routes, lanes)
     chosen = jnp.where(named & (rank == 3 * core + (line >> 2)), 1.0, 0.0)
     picks = jnp.concatenate(
         [jnp.where((line & 3) == q, chosen, 0.0).astype(bf16) for q in range(4)], axis=0
     )
     rows = jnp.concatenate(quarters(core, both_ref), axis=0)
-    out_ref[...] = lax.dot_general(
+    return lax.dot_general(
         picks, rows, (((0,), (0,)), ((), ())), preferred_element_type=f32
     ).astype(bf16)
 
@@ -99,6 +95,7 @@
     routes_ref,
     weights_ref,
     out_gain_ref,
+    outgoing_ref,
     swap_ref,
     keep_ref,
     combine_ref,
@@ -128,6 +125,7 @@
     first = core == 0
     for copy in copies[:3]:
         copy.wait()
+    outgoing_ref[...] = packed(core, routes[...].T, both_ref, outgoing_ref.shape[0])
     combine_weights(routes, weights, combine_ref)
     gain = own_gain[...]
     rows = (both_ref[core].astype(f32) * gain).astype(bf16)
@@ -306,19 +304,10 @@
 
     routes, route_weights = routes.T, route_weights.T
     both = lax.all_gather(tokens, "core", axis=0)
-    outgoing = call(
-        pack_kernel,
-        shape((sent, 128), bf16),
-        core,
-        routes,
-        both,
-        far=(1,),
-        scratch=[pltpu.VMEM(routes.shape, i32), pltpu.SemaphoreType.DMA],
-    )
-    arrived = exchanged(outgoing, sources)
-    near, kept, weights, later_gain = call(
+    outgoing, near, kept, weights, later_gain = call(
         swap_kernel,
         (
+            shape((sent, 128), bf16),
             shape((2 * features + 2 * half + 8, 1024), bf16),
             shape((lines, half, 256), f32),
             shape((6 * rows, sent), bf16),
@@ -346,6 +335,7 @@
         ],
     )
     far = lax.ppermute(near, "core", swap)
+    arrived = exchanged(outgoing, sources)
 
     parts = call(
         hidden_parts_kernel,

time: 126 us -> 125 us (level)
    pallas_call x7 -> x6, Pallas kernels: 5.23 us -> 4.13 us  [call(): pl.pallas_call(body, out_shape=out, in_specs=[spec(n, a) for n, a in enum...]
  transfers between devices with their start and end apart: 1 -> 1, of which waited for: 0 -> 0; matrix products, arithmetic and copies ran while one was open for 0% -> 0% of each run, Pallas kernels for 1% -> 0%
where the time goes in v8:
time: 125 us; the launch traced here: 124 us
  blocking collectives  118 us (94%)
  Pallas kernels  4.13 us (3%)
  starting transfers between devices  2.26 us (2%)
    all_to_all x2, blocking collectives, exchanged(): return lax.all_to_all(blocks, 'ep', 0, 0, tiled=True).reshape(rows.shape)  39.7 us
    all_to_all x1, blocking collectives, per_device(): parts = lax.all_to_all(parts, 'x', 0, 0, tiled=True)  28.5 us
    all_gather x1, blocking collectives, per_device(): hidden = lax.all_gather(hidden, ('x', 'core'), axis=0)  21 us
    all_gather x1, blocking collectives, per_device(): both = lax.all_gather(tokens, 'core', axis=0)  15.8 us
    all_to_all x1, blocking collectives, per_device(): squares = lax.all_to_all(squares, ('x', 'core'), 0, 0, tiled=True)  13 us
    pallas_call x6, Pallas kernels, call(): pl.pallas_call(body, out_shape=out, in_specs=[spec(n, a) for n, a in enum...  4.13 us
  transfers between devices with their start and end apart: 1, of which 0 were waited for; matrix products, arithmetic and copies ran while one was open for 0% of the time, Pallas kernels for 0%

profile of v8, /device:TPU:1, one launch (start us, length us, event | category | flops | bytes accessed | tf_op | source)
XLA Modules:
  0.0 124.4 jit_solution(3334809057215477114)
XLA Ops:
  0.0 15.8 %all-gather = bf16[64,256]{1,0:T(8,128)(2,1)S(1)} all-gather(bf16[32,256]{1,0:T(8,128)(2,1)} %param.11), channel_id=2, replica_groups=mesh['ep'=64,'x'=8,'core'=2] {'core'}, dimensions={0}, use_global_device_ids=true | all-gather | bytes 49152 | tf_op jit(solution)/shard_map/all_gather | solution.py:306
  15.8 0.0 copy-start.2
  15.8 1.9 %shard_map.109 = (bf16[768,128]{1,0:T(8,128)(2,1)S(1)}, bf16[552,1024]{1,0:T(8,128)(2,1)S(1)}, f32[8,16,256]{2,1,0:T(8,128)S(1)}, bf16[192,768]{1,0:T(8,128)(2,1)S(1)}, f32[1,256]{1,0:T(1,128)S(1)}) custom-call(s32[1]{0:T(128)} %bitcast.core_ref, bf16[2,32,256]{2,1,0:T(8,128)(2,1)S(1)} %bitcast.18, f32[1,256]{1,0:T(1,128)} %bitcast.22, ...), custom_call_target="tpu_custom_call" | custom-call | flops 33554432 | bytes 3888132 | tf_op jit(solution)/shard_map/pallas_call | solution.py:262
  17.7 2.3 %collective-permute-start = (bf16[552,1024]{1,0:T(8,128)(2,1)S(1)}, bf16[552,1024]{1,0:T(8,128)(2,1)S(1)}, u32[]{:S(2)}, u32[]{:S(2)}) collective-permute-start(bf16[552,1024]{1,0:T(8,128)(2,1)S(1)} %get-tuple-element.15.near_ref), channel_id=1, source_target_pairs={{0,1},{1,0},{2,3},{3,2},{4,5},{5,4},{6,7},{7,6},{8,9},{9,8},{10,11... | collective-permute-start | bytes 3391496 | tf_op jit(solution)/shard_map/ppermute | solution.py:337
  19.9 22.7 %all_to_all.20 = bf16[64,3,4,128]{3,2,1,0:T(4,128)(2,1)S(1)} all-to-all(bf16[64,3,4,128]{3,2,1,0:T(4,128)(2,1)S(1)} %bitcast.20), channel_id=1, replica_groups=mesh['ep'=64,'x'=8,'core'=2] {'ep'}, dimensions={0} | all-to-all | bytes 393216 | tf_op jit(solution)/shard_map/all_to_all | solution.py:279
  42.6 0.0 collective-permute-done.far_ref
  42.6 0.0 copy-done.2
  42.6 0.6 shard_map.110
  43.2 28.5 %all_to_all.21.parts_ref = bf16[8,216,256]{2,1,0:T(8,128)(2,1)S(1)} all-to-all(bf16[8,216,256]{2,1,0:T(8,128)(2,1)S(1)} %shard_map.110), channel_id=1, replica_groups=mesh['ep'=64,'x'=8,'core'=2] {'x'}, dimensions={0} | all-to-all | bytes 1769472 | tf_op jit(solution)/shard_map/all_to_all | solution.py:353
  71.7 0.0 copy-start
  71.7 0.0 copy-start.1
  71.7 0.2 shard_map.111
  71.9 21.0 %all-gather.1 = bf16[3328,128]{1,0:T(8,128)(2,1)S(1)} all-gather(bf16[208,128]{1,0:T(8,128)(2,1)S(1)} %shard_map.111), channel_id=3, replica_groups=mesh['ep'=64,'x'=8,'core'=2] {'x','core'}, dimensions={0}, use_global_device_ids=true | all-gather | bytes 905216 | tf_op jit(solution)/shard_map/all_gather | solution.py:355
  92.9 0.0 copy-done
  92.9 0.0 copy-done.1
  92.9 0.5 shard_map.112
  93.3 17.0 %all_to_all.22 = bf16[64,3,4,128]{3,2,1,0:T(4,128)(2,1)S(1)} all-to-all(bf16[64,3,4,128]{3,2,1,0:T(4,128)(2,1)S(1)} %bitcast.21), channel_id=1, replica_groups=mesh['ep'=64,'x'=8,'core'=2] {'ep'}, dimensions={0} | all-to-all | bytes 393216 | tf_op jit(solution)/shard_map/all_to_all | solution.py:279
  110.4 0.3 shard_map.113
  110.7 13.0 %all_to_all.23.squares_ref = f32[16,1,128]{2,1,0:T(1,128)S(1)} all-to-all(f32[16,1,128]{2,1,0:T(1,128)S(1)} %get-tuple-element.20), channel_id=1, replica_groups=mesh['ep'=64,'x'=8,'core'=2] {'x','core'}, dimensions={0} | all-to-all | bytes 16384 | tf_op jit(solution)/shard_map/all_to_all | solution.py:373
  123.7 0.7 shard_map.114
Async XLA Ops:
  15.8 26.8 %copy-start.2 = (f32[256]{0:T(256)S(1)}, f32[256]{0:T(256)}, u32[]{:S(2)}) copy-start(f32[256]{0:T(256)} %param.12) | copy-start | bytes 3076
  17.7 24.9 %collective-permute-start = (bf16[552,1024]{1,0:T(8,128)(2,1)S(1)}, bf16[552,1024]{1,0:T(8,128)(2,1)S(1)}, u32[]{:S(2)}, u32[]{:S(2)}) collective-permute-start(bf16[552,1024]{1,0:T(8,128)(2,1)S(1)} %get-tuple-element.15.near_ref), channel_id=1, source_target_pairs={{0,1},{1,0},{2,3},{3,2},{4,5},{5,4},{6,7},{7,6},{8,9},{9,8},{10,11... | collective-permute-start | bytes 3391496 | tf_op jit(solution)/shard_map/ppermute | solution.py:337
  71.7 21.2 %copy-start = (bf16[1,1024,256]{2,1,0:T(8,128)(2,1)S(1)}, bf16[1,1024,256]{2,1,0:T(8,128)(2,1)}, u32[]{:S(2)}) copy-start(bf16[1,1024,256]{2,1,0:T(8,128)(2,1)} %param.17) | copy-start | bytes 1572868
  71.7 21.2 %copy-start.1 = (bf16[1024,256]{1,0:T(8,128)(2,1)S(1)}, bf16[1024,256]{1,0:T(8,128)(2,1)}, u32[]{:S(2)}) copy-start(bf16[1024,256]{1,0:T(8,128)(2,1)} %shared_down_ref.1) | copy-start | bytes 1572868
